TPU v7x, 32 devices: a whole 2x2x4 slice. The times are simulated.
32 devices in a mesh: sp: 4 (over x, core), dp: 8 (over z, y).
Axes of the slice: x: 2, y: 2, z: 4, core: 2. Of those that a mesh axis runs over, the one named last changes fastest.
Arguments:
- content_features_raw: bfloat16 [8, 512, 3072], P('dp', 'sp'), may hold values from -6 to 6
- memory_entering_matrix: bfloat16 [8, 512, 2048], P('dp', 'sp'), may hold values from -6 to 6
- memory_leaving_matrix: bfloat16 [8, 512, 2048], P('dp', 'sp'), may hold values from -6 to 6
- feature_switch_signal: bfloat16 [8, 512, 3072], P('dp', 'sp'), may hold values from -6 to 6
- ahead_increment_raw: float32 [8, 512, 48], P('dp', 'sp'), may hold values from -5 to 5
- reverse_increment_raw: float32 [8, 512, 48], P('dp', 'sp'), may hold values from -5 to 5
- additional_fading: float32 [8, 512, 48], P('dp', 'sp'), as said below
- content_filter_weights: bfloat16 [4, 3072], P(None, 'sp'), may hold values from -3 to 3
- entering_filter_weights: bfloat16 [4, 2048], P(None, 'sp'), may hold values from -3 to 3
- leaving_filter_weights: bfloat16 [4, 2048], P(None, 'sp'), may hold values from -3 to 3
- increment_offset_lanes: float32 [2, 48], P(None, 'sp'), may hold values from -0.5 to 0.5
- fading_speed_exponents: float32 [2, 48], P(None, 'sp'), as said below
- result_scaling_factor: bfloat16 [3072], replicated, may hold values from 0.099609375 to 1.8984375
Outputs:
- out: bfloat16 [8, 512, 3072], P('dp', 'sp')
Inputs may be any that keep to these rules, and one draw needn't show every extreme that they name: Each head's row has a rate exp(fading_speed_exponents) between 0.3 / 4096 and 0.05. `additional_fading`: zero at most positions; elsewhere between log(0.5) and log(0.8).
All inputs are finite; a program needn't handle non-finite values.
Results may differ from a plain program's by a relative error of at most 0.0051.
Values may be sent and summed in bfloat16 or wider, within the bound.
A program may use at most 64 MiB of HBM per device.

v0:
```python
import functools

import jax
import jax.numpy as jnp
from jax import lax
from jax.experimental import pallas as pl
from jax.experimental.pallas import tpu as pltpu
from jax.sharding import PartitionSpec as P

F32 = jnp.float32
BF16 = jnp.bfloat16
HEAD_DIM = 64
STATE = 128
EDGE = 8
HIGHEST = lax.Precision.HIGHEST


def levels_of(sp, dp, groups):
    found = []
    split = 1
    core = 2 if sp % 2 == 0 else 1
    inner = 2 if dp % 2 == 0 and groups % (2 * sp) == 0 else 1
    for axis, count, stride in (("sp", core, 1), ("sp", sp // core, core), ("dp", inner, 1)):
        if count > 1:
            found.append((axis, count, stride))
            split *= count
    return tuple(found), ("dp", dp // inner, inner)


def digit_of(level):
    axis, count, stride = level
    return lax.rem(lax.axis_index(axis) // stride, count)


def member_id(level, member):
    axis, count, stride = level
    return {axis: lax.axis_index(axis) + (member - digit_of(level)) * stride}


def kernel(levels, top, sizes, *refs):
    heads, pairs, chunks, sp, dp = sizes
    (x_ref, b_ref, c_ref, z_ref, ahead_ref, back_ref, spike_ref) = refs[:7]
    params = refs[7:12]
    gain_ref, out_ref = refs[12:14]
    (xc, bc, cc, y_ref, cum_ref, rate_ref, cum_t, rate_t, fac_ref) = refs[14:23]
    refs = refs[:14] + refs[23:]
    got, w_ref, prm_ref, halo_ref, edges, early_sem, edge_sem = (
        refs[14:19], refs[19], refs[20], refs[21], refs[22:28], refs[28], refs[29]
    )
    rest = list(refs[30:])
    depth = len(levels)
    logs = [rest.pop(0) for _ in range(depth + 1)]
    up_log = [rest.pop(0) for _ in range(depth + 1)]
    decay = [rest.pop(0) for _ in range(depth + 1)]
    log_sem = [rest.pop(0) for _ in range(depth + 1)]
    totals, up, down, stage, sems, incoming = ([] for _ in range(6))
    for _ in range(chunks):
        totals.append([rest.pop(0) for _ in range(depth + 1)])
        up.append([rest.pop(0) for _ in range(depth + 1)])
        down.append([rest.pop(0) for _ in range(depth)])
        stage.append([rest.pop(0) for _ in range(depth)])
        sems.append([rest.pop(0) for _ in range(depth + 1)])
        incoming.append(rest.pop(0))
    blk = x_ref.shape[0]
    per_pair = heads // pairs
    x_w = per_pair * HEAD_DIM
    b_w = 2 * STATE
    tiles = x_w // 128
    lane = lax.broadcasted_iota(jnp.int32, (blk, 128), 1)
    left = lane < HEAD_DIM
    row = lax.broadcasted_iota(jnp.int32, (blk, 128), 0)

    segment = ("sp", sp, 1)
    here, there = lax.axis_index("sp"), lax.axis_index("dp")
    rank = there * sp + here
    has_next, has_prev = rank < sp * dp - 1, rank > 0
    after = {"sp": lax.rem(here + 1, sp), "dp": lax.rem(there + (here + 1) // sp, dp)}
    before = {
        "sp": lax.rem(here + sp - 1, sp),
        "dp": lax.rem(there + dp - (sp - here) // sp, dp),
    }
    mesh_id = pl.DeviceIdType.MESH
    barrier = pltpu.get_barrier_semaphore()
    greeted = 0
    for level in levels + (top, segment):
        me = digit_of(level)
        for o in range(1, level[1]):
            target = member_id(level, lax.rem(me + o, level[1]))
            pl.semaphore_signal(barrier, inc=1, device_id=target, device_id_type=mesh_id)
            greeted += 1
    for present, target in ((has_next, after), (has_prev, before)):

        @pl.when(present)
        def _(target=target):
            pl.semaphore_signal(barrier, inc=1, device_id=target, device_id_type=mesh_id)

    filler = jnp.zeros((128 - 2 * heads, blk), F32)
    inc = jnp.concatenate([ahead_ref[...], back_ref[...], filler], axis=0).T
    spikes = jnp.concatenate([spike_ref[...], spike_ref[...], filler], axis=0).T
    count = sp * dp
    neighbours = (rank + count - 1) // count + (2 * count - 2 - rank) // count
    pl.semaphore_wait(barrier, greeted + neighbours)

    def edge_copy(i, direction):
        src = (x_ref, b_ref, c_ref)[i]
        start = blk - EDGE if direction == 0 else 0
        return pltpu.make_async_remote_copy(
            src_ref=src.at[pl.ds(start, EDGE), :],
            dst_ref=edges[3 * direction + i],
            send_sem=edge_sem.at[0, direction, i],
            recv_sem=edge_sem.at[1, direction, i],
            device_id=(after, before)[direction],
            device_id_type=mesh_id,
        )

    def param_copy(i, member, slot):
        return pltpu.make_async_remote_copy(
            src_ref=params[i],
            dst_ref=got[i].at[slot],
            send_sem=early_sem.at[0, i, member],
            recv_sem=early_sem.at[1, i, slot],
            device_id=member_id(segment, member),
            device_id_type=mesh_id,
        )

    for o in range(1, sp):
        for i in range(5):
            param_copy(i, lax.rem(here + o, sp), here).start()
    for direction, present in ((0, has_next), (1, has_prev)):

        @pl.when(present)
        def _(direction=direction):
            for i in range(3):
                edge_copy(i, direction).start()

    for i in range(5):
        got[i][here] = params[i][...]
    for o in range(1, sp):
        for i in range(5):
            s = lax.rem(here + o, sp)
            param_copy(i, s, s).wait_recv()
    prm_ref[...] = jnp.zeros_like(prm_ref)
    wide = got[3].shape[2]
    for q in range(sp):
        for kind in range(2):
            for d in range(2):
                at = slice(d * heads + q * wide, d * heads + (q + 1) * wide)
                prm_ref[kind : kind + 1, at] = got[3 + kind][q, d : d + 1, :]
        off = 0
        for i in range(3):
            n = got[i].shape[2]
            w_ref[0:4, off + q * n : off + (q + 1) * n] = got[i][q].astype(F32)
            off += n * sp
    rate = jax.nn.softplus(inc + prm_ref[0:1, :])
    log_decay = -jnp.exp(prm_ref[1:2, :]) * rate + spikes
    lower = (lane <= row).astype(F32)
    upper = (lane >= row).astype(F32)
    cum_f = jnp.dot(lower, log_decay, precision=HIGHEST, preferred_element_type=F32)
    cum_b = jnp.dot(upper, log_decay, precision=HIGHEST, preferred_element_type=F32)
    cum = jnp.where(lane < heads, cum_f, cum_b)
    lane1 = lane[0:1]
    last = jnp.where(lane1 < heads, cum_f[blk - 1 : blk], cum_b[0:1])
    cum_ref[...] = cum
    rate_ref[...] = rate
    cum_t[...] = cum.T
    rate_t[...] = rate.T
    fac_ref[...] = rate * jnp.exp(last - cum)
    logs[0][...] = jnp.broadcast_to(last, (8, 128))

    def rolled(ref, p):
        return pltpu.roll(ref[...], lax.rem(128 - p * per_pair, 128), 1)

    def two(cols, i):
        return jnp.where(left, cols[:, i : i + 1], cols[:, i + 1 : i + 2])

    def conv(src, col, width, off):
        at = pl.ds(pl.multiple_of(off + col, 128), width)
        v = src[:, pl.ds(pl.multiple_of(col, 128), width)].astype(F32)
        r = lax.broadcasted_iota(jnp.int32, (blk, width), 0)
        h0, h1, h2 = halo_ref[0:1, at], halo_ref[1:2, at], halo_ref[2:3, at]
        m1 = jnp.where(r == 0, h1, pltpu.roll(v, 1, 0))
        m2 = jnp.where(r == 0, h0, jnp.where(r == 1, h1, pltpu.roll(v, 2, 0)))
        p1 = jnp.where(r == blk - 1, h2, pltpu.roll(v, blk - 1, 0))
        s = m2 * w_ref[0:1, at] + m1 * w_ref[1:2, at] + v * w_ref[2:3, at] + p1 * w_ref[3:4, at]
        return (s / (1.0 + jnp.exp(-s))).astype(BF16)

    share = pairs // chunks
    x_total = x_ref.shape[1]
    b_total = b_ref.shape[1]

    def first(c, p, _):
        x_at = pl.ds(pl.multiple_of(p * x_w, 128), x_w)
        b_at = pl.ds(pl.multiple_of(p * b_w, 128), b_w)
        xv = conv(x_ref, p * x_w, x_w, 0)
        bv = conv(b_ref, p * b_w, b_w, x_total)
        xc[:, x_at] = xv
        bc[:, b_at] = bv
        cc[:, b_at] = conv(c_ref, p * b_w, b_w, x_total + b_total)
        cols = rolled(fac_ref, p)
        xf = xv.astype(F32)
        for d in range(2):
            scaled = jnp.concatenate(
                [
                    (xf[:, k * 128 : (k + 1) * 128] * two(cols, d * heads + 2 * k)).astype(BF16)
                    for k in range(tiles)
                ],
                axis=1,
            )
            u = lax.dot_general(scaled, bv, (((0,), (0,)), ((), ())), preferred_element_type=F32)
            half = x_w // 2
            rows = pl.ds(pl.multiple_of((p - c * share) * x_w, 128), x_w)
            totals[c][0][d, rows, :] = jnp.concatenate(
                [u[:half, :STATE], u[half:, STATE:]], axis=0
            ).astype(BF16)
        return 0

    for direction, present in ((0, has_prev), (1, has_next)):

        @pl.when(present)
        def _(direction=direction):
            for i in range(3):
                edge_copy(i, direction).wait_recv()

    off = 0
    for i in range(3):
        n = edges[i].shape[1]
        low = edges[i][...].astype(F32)
        high = edges[3 + i][...].astype(F32)
        halo_ref[0:2, off : off + n] = jnp.where(has_prev, low[EDGE - 2 :], 0.0)
        halo_ref[2:3, off : off + n] = jnp.where(has_next, high[0:1], 0.0)
        off += n
    def inner(p, _):
        x_at = pl.ds(pl.multiple_of(p * x_w, 128), x_w)
        b_at = pl.ds(pl.multiple_of(p * b_w, 128), b_w)
        bv, cv, xv = bc[:, b_at], cc[:, b_at], xc[:, x_at]
        cols = rolled(cum_ref, p)
        parts = []
        for g in range(2):
            scores = lax.dot_general(
                cv[:, g * STATE : (g + 1) * STATE],
                bv[:, g * STATE : (g + 1) * STATE],
                (((1,), (1,)), ((), ())),
                preferred_element_type=F32,
            )
            for i in range(per_pair // 2):
                h = g * (per_pair // 2) + i
                hf = p * per_pair + h
                gap_f = cols[:, h : h + 1] - cum_t[pl.ds(hf, 1), :]
                gap_b = cols[:, heads + h : heads + h + 1] - cum_t[pl.ds(heads + hf, 1), :]
                gap = jnp.where(lane < row, gap_f, jnp.where(lane > row, gap_b, 0.0))
                rf, rb = rate_t[pl.ds(hf, 1), :], rate_t[pl.ds(heads + hf, 1), :]
                scale = jnp.where(lane < row, rf, jnp.where(lane > row, rb, rf + rb))
                parts.append((scores * jnp.exp(gap) * scale).astype(BF16))
        for k in range(tiles):
            xt = xv[:, k * 128 : (k + 1) * 128]
            zero = jnp.zeros_like(xt)
            both = jnp.concatenate([jnp.where(left, xt, zero), jnp.where(left, zero, xt)], axis=0)
            w = jnp.concatenate([parts[2 * k], parts[2 * k + 1]], axis=1)
            y_ref[:, pl.ds(pl.multiple_of(p * x_w + k * 128, 128), 128)] = jnp.dot(
                w, both, preferred_element_type=F32
            )
        return 0

    def copy(src, dst, send, recv, level, member):
        return pltpu.make_async_remote_copy(
            src_ref=src,
            dst_ref=dst,
            send_sem=send,
            recv_sem=recv,
            device_id=member_id(level, member),
            device_id_type=pl.DeviceIdType.MESH,
        )

    every_level = levels + (top,)
    head_share = heads // chunks
    bases = [jnp.int32(0)]
    size = head_share
    for level in levels:
        size = size // level[1]
        bases.append(bases[-1] + digit_of(level) * size)
    pending = [[] for _ in range(chunks)]

    def head_rows(h):
        return pl.ds(pl.multiple_of(h * HEAD_DIM, HEAD_DIM), HEAD_DIM)

    def log_copy(k, member, slot):
        sem = log_sem[k]
        return copy(
            logs[k], up_log[k].at[slot], sem.at[0, member], sem.at[1, slot], every_level[k], member
        )

    def start_up(c, k):
        level = every_level[k]
        n, me = level[1], digit_of(level)
        total, sem = totals[c][k], sems[c][k]
        rows = total.shape[1] // n
        for o in range(1, n):
            m = lax.rem(me + o, n)
            if c == 0:
                pending[c].append(log_copy(k, m, me))
            if k < depth:
                part = total.at[:, pl.ds(pl.multiple_of(m * rows, 64), rows), :]
            else:
                part = total.at[jnp.where(m < me, 1, 0)]
            pending[c].append(
                copy(part, up[c][k].at[me], sem.at[0, m], sem.at[1, me], level, m)
            )
        for one in pending[c]:
            one.start()
        if k < depth:
            up[c][k][me] = total[:, pl.ds(pl.multiple_of(me * rows, 64), rows), :]
        if c == 0:
            up_log[k][me] = logs[k][...]

    def flush(c):
        for one in pending[c]:
            one.wait_send()
        pending[c].clear()

    def finish_up(c, k):
        level = every_level[k]
        n, me = level[1], digit_of(level)
        total, sem = totals[c][k], sems[c][k]
        flush(c)
        for o in range(1, n):
            s = lax.rem(me + o, n)
            if c == 0:
                log_copy(k, s, s).wait_recv()
            part = total.at[:, pl.ds(0, total.shape[1] // n), :] if k < depth else total.at[0]
            copy(part, up[c][k].at[s], sem.at[0, s], sem.at[1, s], level, s).wait_recv()
        if c == 0:

            def expand(m, _):
                decay[k][m] = jnp.exp(jnp.broadcast_to(up_log[k][m][0:1, :], (128, 128)).T)
                return 0

            lax.fori_loop(0, n, expand, 0)
            if k < depth:
                log_sum = up_log[k][0]
                for m in range(1, n):
                    log_sum = log_sum + up_log[k][m]
                logs[k + 1][...] = log_sum

    def gather(c, k):
        n = levels[k][1]
        base = c * head_share + bases[k + 1]
        part, new = up[c][k], totals[c][k + 1]

        def one_head(h, _):
            at = head_rows(h)
            f = part[0, 0, at, :].astype(F32)
            b = part[n - 1, 1, at, :].astype(F32)
            for m in range(1, n):
                r = n - 1 - m
                f = f * decay[k][m, pl.ds(base + h, 1), :] + part[m, 0, at, :].astype(F32)
                b = b * decay[k][r, pl.ds(heads + base + h, 1), :] + part[r, 1, at, :].astype(F32)
            new[0, at, :] = f.astype(BF16)
            new[1, at, :] = b.astype(BF16)
            return 0

        lax.fori_loop(0, new.shape[1] // HEAD_DIM, one_head, 0)

    def enter(c):
        n, me = top[1], digit_of(top)
        base = c * head_share + bases[-1]
        into = incoming[c]
        into[...] = jnp.zeros_like(into)

        def carry(s, d):
            def one_head(h, _):
                at = head_rows(h)
                factor = decay[depth][s, pl.ds(d * heads + base + h, 1), :]
                into[d, at, :] = into[d, at, :] * factor + up[c][depth][s, at, :].astype(F32)
                return 0

            lax.fori_loop(0, into.shape[1] // HEAD_DIM, one_head, 0)
            return 0

        lax.fori_loop(0, me, lambda s, _: carry(s, 0), 0)
        lax.fori_loop(0, n - 1 - me, lambda i, _: carry(n - 1 - i, 1), 0)

    def start_down(c, k):
        level = levels[k]
        n, me = level[1], digit_of(level)
        sem = sems[c][k]
        rows = totals[c][k].shape[1] // n
        base = c * head_share + bases[k + 1]
        source = incoming[c] if k == depth - 1 else down[c][k + 1]
        part, out = up[c][k], stage[c][k]

        def spread(h, _):
            at = head_rows(h)
            f = source[0, at, :].astype(F32)
            b = source[1, at, :].astype(F32)
            for m in range(n):
                r = n - 1 - m
                out[m, 0, at, :] = f.astype(BF16)
                out[r, 1, at, :] = b.astype(BF16)
                if m < n - 1:
                    f = f * decay[k][m, pl.ds(base + h, 1), :] + part[m, 0, at, :].astype(F32)
                    down_factor = decay[k][r, pl.ds(heads + base + h, 1), :]
                    b = b * down_factor + part[r, 1, at, :].astype(F32)
            return 0

        lax.fori_loop(0, rows // HEAD_DIM, spread, 0)
        mine = pl.ds(pl.multiple_of(me * rows, 64), rows)
        for o in range(1, n):
            m = lax.rem(me + o, n)
            pending[c].append(
                copy(out.at[m], down[c][k].at[:, mine, :], sem.at[2, m], sem.at[3, me], level, m)
            )
        for one in pending[c]:
            one.start()
        down[c][k][:, mine, :] = out[me]

    def finish_down(c, k):
        level = levels[k]
        n, me = level[1], digit_of(level)
        sem = sems[c][k]
        rows = totals[c][k].shape[1] // n
        flush(c)
        for o in range(1, n):
            s = lax.rem(me + o, n)
            theirs = pl.ds(pl.multiple_of(s * rows, 64), rows)
            copy(
                stage[c][k].at[s], down[c][k].at[:, theirs, :], sem.at[2, s], sem.at[3, s], level, s
            ).wait_recv()

    for c in range(chunks):
        lax.fori_loop(c * share, (c + 1) * share, functools.partial(first, c), 0)
        start_up(c, 0)
    for o in range(1, sp):
        for i in range(5):
            param_copy(i, lax.rem(here + o, sp), here).wait_send()
    for direction, present in ((0, has_next), (1, has_prev)):

        @pl.when(present)
        def _(direction=direction):
            for i in range(3):
                edge_copy(i, direction).wait_send()


    gaps = chunks * depth
    cuts = [(i * pairs) // gaps for i in range(gaps + 1)]
    for k in range(depth):
        for c in range(chunks):
            finish_up(c, k)
            gather(c, k)
            start_up(c, k + 1)
            at = k * chunks + c
            lax.fori_loop(cuts[at], cuts[at + 1], inner, 0)
    for c in range(chunks):
        finish_up(c, depth)
        enter(c)
        start_down(c, depth - 1)
    for k in reversed(range(1, depth)):
        for c in range(chunks):
            finish_down(c, k)
            start_down(c, k - 1)

    cum_ref[...] = jnp.exp(cum_ref[...])

    def last_part(c, p, _):
        cv = cc[:, pl.ds(pl.multiple_of(p * b_w, 128), b_w)]
        cols = rolled(cum_ref, p)
        carried = []
        for d in range(2):
            st = down[c][0][d, pl.ds(pl.multiple_of((p - c * share) * x_w, 128), x_w), :]
            got = [
                lax.dot_general(
                    cv[:, g * STATE : (g + 1) * STATE],
                    st,
                    (((1,), (1,)), ((), ())),
                    preferred_element_type=F32,
                )
                for g in range(2)
            ]
            carried.append(got)
        for k in range(tiles):
            cut = slice(k * 128, (k + 1) * 128)
            at = pl.ds(pl.multiple_of(p * x_w + k * 128, 128), 128)
            y = y_ref[:, at]
            for d in range(2):
                a, b = carried[d][0][:, cut], carried[d][1][:, cut]
                if 2 * k + 1 < per_pair // 2:
                    v = a
                elif 2 * k >= per_pair // 2:
                    v = b
                else:
                    v = jnp.where(left, a, b)
                y = y + v * two(cols, d * heads + 2 * k)
            z = z_ref[:, at].astype(F32)
            gated = y.astype(BF16).astype(F32) * (z / (1.0 + jnp.exp(-z)))
            square = gated * gated
            low = jnp.sum(jnp.where(left, square, 0.0), axis=1, keepdims=True)
            high = jnp.sum(jnp.where(left, 0.0, square), axis=1, keepdims=True)
            mean = jnp.where(left, low, high) * (1.0 / HEAD_DIM)
            out_ref[:, at] = (gated * lax.rsqrt(mean + 1e-6) * gain_ref[0:1, at]).astype(BF16)
        return 0

    for c in range(chunks):
        finish_down(c, 0)
        lax.fori_loop(c * share, (c + 1) * share, functools.partial(last_part, c), 0)


def local(sp, dp, x, b, c, z, ahead, back, spike, wx, wb, wc, offset, fading, gain):
    x, b, c, z = x[0], b[0], c[0], z[0]
    blk, x_total = x.shape
    groups = b.shape[1] // STATE
    heads = ahead.shape[2]
    pairs = groups // 2
    levels, top = levels_of(sp, dp, groups)
    scratch = [
        pltpu.VMEM((blk, x_total), BF16),
        pltpu.VMEM((blk, groups * STATE), BF16),
        pltpu.VMEM((blk, groups * STATE), BF16),
        pltpu.VMEM((blk, x_total), F32),
    ]
    scratch += [pltpu.VMEM((128, 128), F32)] * 5
    params = (wx, wb, wc, offset, fading)
    width = x_total + 2 * b.shape[1]
    early = [pltpu.VMEM((sp,) + one.shape, one.dtype) for one in params]
    early += [pltpu.VMEM((8, width), F32), pltpu.VMEM((8, 128), F32), pltpu.VMEM((8, width), F32)]
    early += [pltpu.VMEM((EDGE, one.shape[1]), BF16) for one in (x, b, c)] * 2
    early += [pltpu.SemaphoreType.DMA((2, 5, sp)), pltpu.SemaphoreType.DMA((2, 2, 3))]
    scratch += early
    split = 1
    for level in levels:
        split *= level[1]
    chunks = 2 if groups % (2 * split) == 0 else 1
    counts = [level[1] for level in levels] + [top[1]]
    scratch += [pltpu.VMEM((8, 128), F32)] * len(counts)
    scratch += [pltpu.VMEM((n, 8, 128), F32) for n in counts]
    scratch += [pltpu.VMEM((n, 128, 128), F32) for n in counts]
    scratch += [pltpu.SemaphoreType.DMA((2, n)) for n in counts]
    for _ in range(chunks):
        held = [x_total // chunks]
        for n in counts[:-1]:
            held.append(held[-1] // n)
        slabs = list(zip(counts[:-1], held[1:]))
        scratch += [pltpu.VMEM((2, rows, STATE), BF16) for rows in held]
        scratch += [pltpu.VMEM((n, 2, rows, STATE), BF16) for n, rows in slabs]
        scratch += [pltpu.VMEM((counts[-1], held[-1], STATE), BF16)]
        scratch += [pltpu.VMEM((2, rows, STATE), BF16) for rows in held[:-1]]
        scratch += [pltpu.VMEM((n, 2, rows, STATE), BF16) for n, rows in slabs]
        scratch += [pltpu.SemaphoreType.DMA((4, n)) for n in counts]
        scratch += [pltpu.VMEM((2, held[-1], STATE), F32)]
    out = pl.pallas_call(
        functools.partial(kernel, levels, top, (heads, pairs, chunks, sp, dp)),
        out_shape=jax.ShapeDtypeStruct((blk, x_total), BF16),
        in_specs=[pl.BlockSpec(memory_space=pltpu.VMEM)] * 13,
        out_specs=pl.BlockSpec(memory_space=pltpu.VMEM),
        scratch_shapes=scratch,
        compiler_params=pltpu.CompilerParams(
            collective_id=0, has_side_effects=True, vmem_limit_bytes=60 * 2**20
        ),
        name="mixer",
    )(x, b, c, z, ahead[0].T, back[0].T, spike[0].T, *params, gain.astype(F32)[None])
    return out[None]


def solution(mesh):
    tokens = P("dp", "sp", None)
    placed = (tokens,) * 7 + (P(None, "sp"),) * 5 + (P(),)
    return jax.shard_map(
        functools.partial(local, mesh.shape["sp"], mesh.shape["dp"]),
        mesh=mesh,
        in_specs=placed,
        out_specs=tokens,
        check_vma=False,
    )
```

profile of v0, /device:TPU:8, one launch (start us, length us, event | category | flops | bytes accessed | tf_op | source)
XLA Modules:
  0.0 61.8 jit_solution(17215395492030648556)
XLA Ops:
  0.0 0.0 copy-start
  0.0 0.7 %copy-done = bf16[3072]{0:T(1024)(128)(2,1)S(1)} copy-done((bf16[3072]{0:T(1024)(128)(2,1)S(1)}, bf16[3072]{0:T(1024)(128)(2,1)}, u32[]{:S(2)}) %copy-start) | copy-done | bytes 6168
  0.7 0.6 broadcast_in_dim.11
  1.3 58.5 %mixer.1 = bf16[128,3072]{1,0:T(8,128)(2,1)} custom-call(bf16[128,3072]{1,0:T(8,128)(2,1)} %bitcast.16, bf16[128,2048]{1,0:T(8,128)(2,1)} %bitcast.18, bf16[128,2048]{1,0:T(8,128)(2,1)} %bitcast.19, bf16[128,3072]{1,0:T(8,128)(2,1)} %bitcast.17, f32[48,128]{1,0:T(8,128)} %bitcast.21, f32[48,128]{1,0:T(8,128)} %bitcast.22, f32[48,128]{1,0:T(8,128)} %bitcast.23, ...), custom_call_target="tpu_custom_call" | custom-call | tf_op jit(solution)/shard_map/mixer/pallas_call | solution.py:548
  59.8 2.1 %copy.15 = bf16[1,128,3072]{2,1,0:T(8,128)(2,1)} copy(bf16[1,128,3072]{2,1,0:T(8,128)(2,1)} %bitcast.15) | data formatting | bytes 1572864
Async XLA Ops:
  0.0 0.7 %copy-start = (bf16[3072]{0:T(1024)(128)(2,1)S(1)}, bf16[3072]{0:T(1024)(128)(2,1)}, u32[]{:S(2)}) copy-start(bf16[3072]{0:T(1024)(128)(2,1)} %param.25) | copy-start | bytes 18436
where the time goes:
time: 62.1 us; the launch traced here: 61.8 us
  Pallas kernels  58.5 us (94%)
  local copies, waits for them, and re-layouts  2.75 us (4%)
    pallas_call x1, Pallas kernels, local(): pl.pallas_call(functools.partial(kernel, levels, top, (heads, pairs, chun...  58.5 us
    unnamed x3, local copies, waits for them, and re-layouts  2.75 us

commit v1 on v0

--- a/solution.py
+++ b/solution.py
@@ -559,11 +559,708 @@
     return out[None]
 
 
+def quad_kernel(sizes, *refs):
+    heads, pairs, sp, dp = sizes
+    nz = dp // 2
+    rounds = nz.bit_length() - 1
+    (x_hbm, b_hbm, c_hbm, z_hbm, ahead_hbm, back_hbm, spike_hbm) = refs[:7]
+    params = refs[7:12]
+    gain_hbm, out_hbm = refs[12:14]
+    (in_x, in_b, in_c, in_z, inc, inc_out, gain_in, px, pb, pc) = refs[14:24]
+    own, got = refs[24:29], refs[29:34]
+    edges = refs[34:40]
+    (work, w_ref, prm_ref, gain_ref, cum_ref, fac_ref, col_ref, cum_t, rate_t, mid_t) = refs[40:50]
+    (xc, bt, cc, y_ref, sup, up_in, down_out, down_in) = refs[50:58]
+    (logs, qlog, zsum, zlog, dec, wup, zdec, zwt) = refs[58:66]
+    (tz, zin, zs, zr, mix_out, mix_in, out_v) = refs[66:73]
+    (load_sem, prm_sem, edge_sem, half_sem, inc_sem, qlog_sem, zlog_sem) = refs[73:80]
+    (up_sem, zsend_sem, zrecv_sem, down_sem, mix_sem, out_sem) = refs[80:86]
+
+    hh = heads // 2
+    hp = pairs // 2
+    per_pair = heads // pairs
+    tiles = per_pair * HEAD_DIM // 128
+    blk = in_x.shape[0]
+    tokens = 2 * blk
+    x_half = in_x.shape[1] // 2
+    b_half = in_b.shape[1] // 2
+    x_w = per_pair * HEAD_DIM
+    mesh_id = pl.DeviceIdType.MESH
+
+    here, there = lax.axis_index("sp"), lax.axis_index("dp")
+    core, cx = lax.rem(here, 2), here // 2
+    cy, cz = lax.rem(there, 2), there // 2
+    other = 1 - core
+    me = cy * 2 + cx
+    chip = there * 2 + cx
+    chips = dp * 2
+    has_next, has_prev = chip < chips - 1, chip > 0
+    after, before = lax.rem(chip + 1, chips), lax.rem(chip + chips - 1, chips)
+    partner = {"sp": cx * 2 + other}
+
+    def chip_id(c, k):
+        return {"sp": lax.rem(c, 2) * 2 + k, "dp": c // 2}
+
+    def quad_id(qy, qx):
+        return {"sp": qx * 2 + core, "dp": cz * 2 + qy}
+
+    def z_id(z):
+        return {"dp": z * 2 + cy}
+
+    def member(i):
+        qy = lax.rem(cy + lax.rem(i + 1, 2), 2)
+        qx = lax.rem(cx + (3 - i) // 2, 2)
+        return qy, qx, qy * 2 + qx
+
+    def remote(src, dst, send, recv, target):
+        return pltpu.make_async_remote_copy(
+            src_ref=src, dst_ref=dst, send_sem=send, recv_sem=recv,
+            device_id=target, device_id_type=mesh_id,
+        )
+
+    barrier = pltpu.get_barrier_semaphore()
+
+    def greet(target):
+        pl.semaphore_signal(barrier, inc=1, device_id=target, device_id_type=mesh_id)
+
+    for o in range(1, sp):
+        greet({"sp": lax.rem(here + o, sp)})
+    for i in range(3):
+        qy, qx, _ = member(i)
+        greet(quad_id(qy, qx))
+    for o in range(1, nz):
+        greet(z_id(lax.rem(cz + o, nz)))
+    for present, neighbour in ((has_next, after), (has_prev, before)):
+
+        @pl.when(present)
+        def _(neighbour=neighbour):
+            for k in range(2):
+                greet(chip_id(neighbour, k))
+
+    loads = []
+
+    def load(src, dst):
+        one = pltpu.make_async_copy(src, dst, load_sem.at[len(loads)])
+        one.start()
+        loads.append(one)
+        return one
+
+    param_loads = [load(params[i], own[i]) for i in range(5)]
+    mine = pl.ds(pl.multiple_of(core * hh, 8), hh)
+    theirs = pl.ds(pl.multiple_of(other * hh, 8), hh)
+    raw = (ahead_hbm, back_hbm, spike_hbm)
+    inc_stage = [load(raw[i].at[theirs, :], inc_out.at[i]) for i in range(3)]
+    inc_loads = [load(raw[i].at[mine, :], inc.at[core, i]) for i in range(3)]
+    b_load = load(b_hbm, in_b)
+    x_load = load(x_hbm, in_x)
+    c_load = load(c_hbm, in_c)
+    gain_load = load(gain_hbm, gain_in)
+    z_load = load(z_hbm, in_z)
+
+    for one in param_loads + inc_stage:
+        one.wait()
+    chip_greets = 2 * ((chip + chips - 1) // chips + (2 * chips - 2 - chip) // chips)
+    pl.semaphore_wait(barrier, (sp - 1) + 3 + (nz - 1) + chip_greets)
+
+    holder = here // 2
+    slot = lax.rem(here, 2)
+
+    def param_copy(i, x):
+        return remote(
+            own[i], got[i].at[slot], prm_sem.at[0, i, x], prm_sem.at[1, i, slot],
+            {"sp": x * 2 + holder},
+        )
+
+    for x in range(2):
+        elsewhere = x * 2 + holder != here
+
+        @pl.when(elsewhere)
+        def _(x=x):
+            for i in range(5):
+                param_copy(i, x).start()
+
+        @pl.when(jnp.logical_not(elsewhere))
+        def _():
+            for i in range(5):
+                got[i][slot] = own[i][...]
+
+    def inc_copy(i):
+        return remote(
+            inc_out.at[i], inc.at[core, i], inc_sem.at[0, i], inc_sem.at[1, i], partner
+        )
+
+    for i in range(3):
+        inc_copy(i).start()
+
+    sources = (in_x, in_b, in_c)
+    halves = (x_half, b_half, b_half)
+
+    def edge_copy(i, low, k):
+        half = halves[i]
+        start = blk - EDGE if low else 0
+        return remote(
+            sources[i].at[pl.ds(start, EDGE), pl.ds(k * half, half)],
+            edges[i if low else 3 + i],
+            edge_sem.at[0, i, k],
+            edge_sem.at[1, i, 0 if low else 1],
+            chip_id(after if low else before, k),
+        )
+
+    sends_low = jnp.logical_and(core == 1, has_next)
+    sends_high = jnp.logical_and(core == 0, has_prev)
+
+    def half_copy(i):
+        cut = pl.ds(pl.multiple_of(other * halves[i], 128), halves[i])
+        return remote(
+            sources[i].at[:, cut], (px, pb, pc)[i], half_sem.at[0, i], half_sem.at[1, i], partner
+        )
+
+    for i, one in ((1, b_load), (0, x_load), (2, c_load)):
+        one.wait()
+
+        @pl.when(sends_low)
+        def _(i=i):
+            for k in range(2):
+                edge_copy(i, True, k).start()
+
+        @pl.when(sends_high)
+        def _(i=i):
+            for k in range(2):
+                edge_copy(i, False, k).start()
+
+        half_copy(i).start()
+
+    lane = lax.broadcasted_iota(jnp.int32, (blk, 128), 1)
+    row = lax.broadcasted_iota(jnp.int32, (blk, 128), 0)
+    left = lane < HEAD_DIM
+    left1 = left[0:1]
+    lower = (lane <= row).astype(F32)
+    upper = (lane >= row).astype(F32)
+    filler = jnp.zeros((128 - 2 * hh, blk), F32)
+
+    for q in range(2):
+        from_q = 2 * core + q != here
+
+        @pl.when(from_q)
+        def _(q=q):
+            for i in range(5):
+                remote(
+                    own[i], got[i].at[q], prm_sem.at[0, i, 0], prm_sem.at[1, i, q], partner
+                ).wait_recv()
+
+    for one in inc_loads:
+        one.wait()
+    for i in range(3):
+        remote(
+            inc_out.at[i], inc.at[other, i], inc_sem.at[0, i], inc_sem.at[1, i], partner
+        ).wait_recv()
+    prm_ref[...] = jnp.zeros_like(prm_ref)
+    wide = own[3].shape[1]
+    for q in range(2):
+        for kind in range(2):
+            for d in range(2):
+                at = slice(d * hh + q * wide, d * hh + (q + 1) * wide)
+                prm_ref[kind : kind + 1, at] = got[3 + kind][q, d : d + 1, :]
+        off = 0
+        for i in range(3):
+            n = own[i].shape[1]
+            w_ref[0:4, off + q * n : off + (q + 1) * n] = got[i][q].astype(F32)
+            off += 2 * n
+
+    cums, rates = [], []
+    for j in range(2):
+        pre = jnp.concatenate([inc[j, 0], inc[j, 1], filler], axis=0).T
+        spikes = jnp.concatenate([inc[j, 2], inc[j, 2], filler], axis=0).T
+        rate = jax.nn.softplus(pre + prm_ref[0:1, :])
+        log_decay = -jnp.exp(prm_ref[1:2, :]) * rate + spikes
+        cum_f = jnp.dot(lower, log_decay, precision=HIGHEST, preferred_element_type=F32)
+        cum_b = jnp.dot(upper, log_decay, precision=HIGHEST, preferred_element_type=F32)
+        cums.append((cum_f, cum_b))
+        rates.append(rate)
+    ahead_lane = lane < hh
+    ahead1 = ahead_lane[0:1]
+    mid_f, mid_b = cums[0][0][blk - 1 : blk], cums[1][1][0:1]
+    total = jnp.where(ahead1, mid_f + cums[1][0][blk - 1 : blk], cums[0][1][0:1] + mid_b)
+    logs[...] = jnp.broadcast_to(total, (8, 128))
+
+    def qlog_copy(i):
+        qy, qx, q = member(i)
+        return remote(
+            logs, qlog.at[me], qlog_sem.at[0, i], qlog_sem.at[1, me], quad_id(qy, qx)
+        )
+
+    for i in range(3):
+        qlog_copy(i).start()
+    qlog[me] = logs[...]
+    for j in range(2):
+        cum_f, cum_b = cums[j]
+        far = jnp.where(ahead_lane, mid_f if j == 1 else 0.0, mid_b if j == 0 else 0.0)
+        near = jnp.where(ahead_lane, cum_f, cum_b)
+        at = slice(j * blk, (j + 1) * blk)
+        cum = near + far
+        cum_ref[at, :] = jnp.exp(cum)
+        fac_ref[at, :] = rates[j] * jnp.exp(total - cum)
+        col_ref[at, :] = cum
+        cum_t[:, at] = cum.T
+        rate_t[:, at] = rates[j].T
+        mid = rates[j] * jnp.exp(jnp.minimum((mid_f if j == 0 else mid_b) - near, 0.0))
+        mid_t[:, at] = mid.T
+
+    for k in range(gain_in.shape[0]):
+        if k == 0:
+            gain_load.wait()
+        gain_ref[0:1, k * 128 : (k + 1) * 128] = gain_in[k : k + 1, :].astype(F32)
+
+    for i in range(3):
+        remote(sources[i].at[:, pl.ds(0, halves[i])], (px, pb, pc)[i], half_sem.at[0, i],
+               half_sem.at[1, i], partner).wait_recv()
+    for low, present in ((True, has_prev), (False, has_next)):
+
+        @pl.when(present)
+        def _(low=low):
+            for i in range(3):
+                edge_copy(i, low, 0).wait_recv()
+
+    def rolled(v, p):
+        return pltpu.roll(v, lax.rem(128 - p * per_pair, 128), 1)
+
+    def two(cols, i):
+        mask = lax.broadcasted_iota(jnp.int32, (cols.shape[0], 128), 1) < HEAD_DIM
+        return jnp.where(mask, cols[:, i : i + 1], cols[:, i + 1 : i + 2])
+
+    offsets = (0, 2 * own[0].shape[1], 2 * own[0].shape[1] + 2 * own[1].shape[1])
+
+    def conv(i, col, spot):
+        half = halves[i]
+        mine_at = pl.ds(pl.multiple_of(core * half + col, 128), 128)
+        at = pl.ds(pl.multiple_of(col, 128), 128)
+        buf = work.at[spot]
+        buf[pl.ds(pl.multiple_of(8 + core * blk, 8), blk), :] = sources[i][:, mine_at].astype(F32)
+        buf[pl.ds(pl.multiple_of(8 + other * blk, 8), blk), :] = (px, pb, pc)[i][:, at].astype(F32)
+        buf[0:8, :] = jnp.where(has_prev, edges[i][:, at].astype(F32), 0.0)
+        high = jnp.where(has_next, edges[3 + i][:, at].astype(F32), 0.0)
+        buf[8 + tokens : 16 + tokens, :] = high
+        w_at = pl.ds(pl.multiple_of(offsets[i] + col, 128), 128)
+        s = buf[6 : 6 + tokens, :] * w_ref[0:1, w_at]
+        for k in range(1, 4):
+            s = s + buf[6 + k : 6 + k + tokens, :] * w_ref[k : k + 1, w_at]
+        h = 0.5 * s
+        return h + h * jnp.tanh(h)
+
+    def up_copy(k, i):
+        qy, qx, q = member(i)
+        return remote(
+            sup.at[k, q], up_in.at[k, me], up_sem.at[0, k, i], up_sem.at[1, k, me],
+            quad_id(qy, qx),
+        )
+
+    def wide_left(n):
+        return lax.rem(lax.broadcasted_iota(jnp.int32, (128, n), 1), 128) < HEAD_DIM
+
+    def first(k, i, _):
+        _, _, p = member(i)
+        if k < 2:
+            g = 2 * p + k
+            bt[g] = conv(1, g * 128, 0).T.astype(BF16)
+        col = p * x_w + k * 128
+        xv = conv(0, col, 1).astype(BF16)
+        xc[:, pl.ds(pl.multiple_of(col, 128), 128)] = xv
+        xf = xv.astype(F32)
+        cols = rolled(fac_ref[...], p)
+        rhs = jnp.concatenate(
+            [(xf * two(cols, d * hh + 2 * k)).astype(BF16) for d in range(2)], axis=1
+        )
+        u = jnp.dot(bt[2 * p + k // 2], rhs, preferred_element_type=F32)
+        if k == 1:
+            v = jnp.dot(bt[2 * p + 1], rhs, preferred_element_type=F32)
+            u = jnp.where(wide_left(256), u, v)
+        u = u.astype(BF16)
+
+        @pl.when(i < 3)
+        def _():
+            sup[k, p, 0] = u[:, :128]
+            sup[k, p, 1] = u[:, 128:]
+            up_copy(k, i).start()
+
+        @pl.when(i == 3)
+        def _():
+            up_in[k, p, 0] = u[:, :128]
+            up_in[k, p, 1] = u[:, 128:]
+
+        return 0
+
+    def inner(p, _):
+        x_at = [pl.ds(pl.multiple_of(p * x_w + k * 128, 128), 128) for k in range(tiles)]
+        for g in range(2):
+            at = pl.ds(pl.multiple_of((2 * p + g) * 128, 128), 128)
+            cc[:, at] = conv(2, (2 * p + g) * 128, g).astype(BF16)
+        for r in range(2):
+            rows = slice(r * blk, (r + 1) * blk)
+            cols = rolled(col_ref[rows, :], p)
+            mid_row = mid_f if r == 1 else mid_b
+            shift = rolled(jnp.exp(jnp.minimum(col_ref[rows, :] - mid_row, 0.0)), p)
+            parts = []
+            for g in range(2):
+                at = pl.ds(pl.multiple_of((2 * p + g) * 128, 128), 128)
+                scores = jnp.dot(cc[rows, at], bt[2 * p + g], preferred_element_type=F32)
+                on = scores[:, r * blk : (r + 1) * blk]
+                away = scores[:, (1 - r) * blk : (2 - r) * blk]
+                for h in range(g * per_pair // 2, (g + 1) * per_pair // 2):
+                    f = pl.ds(p * per_pair + h, 1)
+                    b = pl.ds(hh + p * per_pair + h, 1)
+                    gap_f = cols[:, h : h + 1] - cum_t[f, rows]
+                    gap_b = cols[:, hh + h : hh + h + 1] - cum_t[b, rows]
+                    gap = jnp.where(lane < row, gap_f, jnp.where(lane > row, gap_b, 0.0))
+                    rf, rb = rate_t[f, rows], rate_t[b, rows]
+                    scale = jnp.where(lane < row, rf, jnp.where(lane > row, rb, rf + rb))
+                    near = (on * jnp.exp(gap) * scale).astype(BF16)
+                    d = 1 - r
+                    c = d * hh + h
+                    far_rows = slice((1 - r) * blk, (2 - r) * blk)
+                    far_row = mid_t[f if d == 0 else b, far_rows]
+                    far = (away * shift[:, c : c + 1] * far_row).astype(BF16)
+                    parts.append(jnp.concatenate([near, far] if r == 0 else [far, near], axis=1))
+            for k in range(tiles):
+                xt = xc[:, x_at[k]]
+                zero = jnp.zeros_like(xt)
+                mask = lax.broadcasted_iota(jnp.int32, xt.shape, 1) < HEAD_DIM
+                both = jnp.concatenate(
+                    [jnp.where(mask, xt, zero), jnp.where(mask, zero, xt)], axis=0
+                )
+                w = jnp.concatenate([parts[2 * k], parts[2 * k + 1]], axis=1)
+                y_ref[rows, x_at[k]] = jnp.dot(w, both, preferred_element_type=F32)
+        return 0
+
+    def zlog_copy(o):
+        return remote(
+            zsum, zlog.at[cz], zlog_sem.at[0, o], zlog_sem.at[1, cz], z_id(lax.rem(cz + o, nz))
+        )
+
+    def lanes_of(log_row, d, k):
+        return two(rolled(log_row, me), d * hh + 2 * k)
+
+    def quad_logs():
+        for i in range(3):
+            _, _, q = member(i)
+            remote(
+                logs, qlog.at[q], qlog_sem.at[0, i], qlog_sem.at[1, q], partner
+            ).wait_recv()
+        zsum[...] = qlog[0] + qlog[1] + qlog[2] + qlog[3]
+        for o in range(1, nz):
+            zlog_copy(o).start()
+        zlog[cz] = zsum[...]
+        for d in range(2):
+            for k in range(tiles):
+                each = [lanes_of(qlog[q], d, k) for q in range(4)]
+                reach = jnp.zeros_like(each[0])
+                for q in reversed(range(4)) if d == 0 else range(4):
+                    dec[q, d, k] = jnp.exp(each[q])
+                    wup[q, d, k] = jnp.exp(reach)
+                    reach = reach + each[q]
+
+    def z_logs():
+        for o in range(1, nz):
+            s = lax.rem(cz + o, nz)
+            remote(
+                zsum, zlog.at[s], zlog_sem.at[0, o], zlog_sem.at[1, s], partner
+            ).wait_recv()
+        reach = [[jnp.zeros((8, 128), F32) for _ in range(2)] for _ in range(rounds)]
+        for s in range(nz):
+            for r in range(rounds):
+                h = 1 << r
+                pos = lax.rem(cz, 2 * h)
+                middle = cz - pos + h
+                f_in = jnp.logical_and(s >= middle, s < cz)
+                b_in = jnp.logical_and(s > cz, s < middle)
+                reach[r][0] = reach[r][0] + jnp.where(f_in, zlog[s], 0.0)
+                reach[r][1] = reach[r][1] + jnp.where(b_in, zlog[s], 0.0)
+        for d in range(2):
+            for k in range(tiles):
+                zdec[d, k] = jnp.exp(lanes_of(zsum[...], d, k))
+                for r in range(rounds):
+                    zwt[r, d, k] = jnp.exp(lanes_of(reach[r][d], d, k))
+
+    def combine(k):
+        for i in range(3):
+            _, _, q = member(i)
+            remote(
+                sup.at[k, q], up_in.at[k, q], up_sem.at[0, k, i], up_sem.at[1, k, q], partner
+            ).wait_recv()
+        for d in range(2):
+            acc = up_in[k, 0, d].astype(F32) * wup[0, d, k, 0:1, :]
+            for q in range(1, 4):
+                acc = acc + up_in[k, q, d].astype(F32) * wup[q, d, k, 0:1, :]
+            tz[k, d] = acc
+            zin[k, d] = jnp.zeros_like(acc)
+
+    def z_copy(r, k, o, d):
+        return remote(
+            zs.at[r, k], zr.at[r, k], zsend_sem.at[r, k, o - 1], zrecv_sem.at[r, k],
+            z_id(cz + o if d == 0 else cz - o),
+        )
+
+    def z_parts(r):
+        h = 1 << r
+        pos = lax.rem(cz, 2 * h)
+        return h, pos, ((0, pos == h - 1), (1, pos == h))
+
+    def z_send(r, k):
+        h, pos, senders = z_parts(r)
+        for d, sender in senders:
+
+            @pl.when(sender)
+            def _(d=d):
+                zs[r, k] = (zin[k, d] * zdec[d, k, 0:1, :] + tz[k, d]).astype(BF16)
+                for o in reversed(range(1, h + 1)):
+                    z_copy(r, k, o, d).start()
+
+    def z_recv(r, k):
+        h, pos, _ = z_parts(r)
+        z_copy(r, k, 1, 0).wait_recv()
+        for d, receiver in ((0, pos >= h), (1, pos < h)):
+
+            @pl.when(receiver)
+            def _(d=d):
+                zin[k, d] = zin[k, d] + zr[r, k].astype(F32) * zwt[r, d, k, 0:1, :]
+
+    def down_copy(k, i):
+        qy, qx, q = member(i)
+        return remote(
+            down_out.at[k, q], down_in.at[k, me], down_sem.at[0, k, i], down_sem.at[1, k, me],
+            quad_id(qy, qx),
+        )
+
+    def down(k):
+        for d in range(2):
+            g = zin[k, d]
+            order = list(range(4)) if d == 0 else list(reversed(range(4)))
+            for q in order:
+                down_out[k, q, d] = g.astype(BF16)
+                if q != order[-1]:
+                    g = g * dec[q, d, k, 0:1, :] + up_in[k, q, d].astype(F32)
+        for i in range(3):
+            down_copy(k, i).start()
+        down_in[k, me] = down_out[k, me]
+
+    def gate(mixed, at):
+        z = in_z[:, at].astype(F32)
+        half_z = 0.5 * z
+        gated = mixed.astype(F32) * (half_z + half_z * jnp.tanh(half_z))
+        square = gated * gated
+        low = jnp.sum(jnp.where(left, square, 0.0), axis=1, keepdims=True)
+        high = jnp.sum(jnp.where(left, 0.0, square), axis=1, keepdims=True)
+        mean = jnp.where(left, low, high) * (1.0 / HEAD_DIM)
+        out_v[:, at] = (gated * lax.rsqrt(mean + 1e-6) * gain_ref[0:1, at]).astype(BF16)
+
+    def mix_copy(k, p):
+        return remote(
+            mix_out.at[k, p], mix_in.at[k, p], mix_sem.at[0, k, p], mix_sem.at[1, k, p], partner
+        )
+
+    def last(k, j, _):
+        i = 3 - j
+        _, _, p = member(i)
+
+        @pl.when(i < 3)
+        def _():
+            remote(
+                down_out.at[k, p], down_in.at[k, p], down_sem.at[0, k, i], down_sem.at[1, k, p],
+                partner,
+            ).wait_recv()
+
+        rhs = jnp.concatenate([down_in[k, p, 0], down_in[k, p, 1]], axis=1)
+        at = pl.ds(pl.multiple_of(p * x_w + k * 128, 128), 128)
+        for mine in (False, True):
+            start = pl.multiple_of((core if mine else other) * blk, 128)
+            rows = pl.ds(start, blk)
+            c_at = [pl.ds(pl.multiple_of((2 * p + g) * 128, 128), 128) for g in range(2)]
+            v = jnp.dot(cc[rows, c_at[k // 2]], rhs, preferred_element_type=F32)
+            if k == 1:
+                u = jnp.dot(cc[rows, c_at[1]], rhs, preferred_element_type=F32)
+                v = jnp.where(wide_left(256), v, u)
+            cols = rolled(cum_ref[rows, :], p)
+            y = y_ref[rows, at] + v[:, :128] * two(cols, 2 * k) + v[:, 128:] * two(cols, hh + 2 * k)
+            mixed = y.astype(BF16)
+            if mine:
+                gate(mixed, pl.ds(pl.multiple_of(core * x_half + p * x_w + k * 128, 128), 128))
+            else:
+                mix_out[k, p] = mixed
+                mix_copy(k, p).start()
+        return 0
+
+    def out_copy(k, half, p):
+        at = pl.ds(pl.multiple_of(half * x_half + p * x_w + k * 128, 128), 128)
+        return pltpu.make_async_copy(out_v.at[:, at], out_hbm.at[:, at], out_sem.at[k, half, p])
+
+    def take(k, p, _):
+        mix_copy(k, p).wait_recv()
+        gate(mix_in[k, p], pl.ds(pl.multiple_of(other * x_half + p * x_w + k * 128, 128), 128))
+        return 0
+
+    def finish(k):
+        lax.fori_loop(0, hp, functools.partial(take, k), 0)
+        for half in range(2):
+            for p in range(hp):
+                out_copy(k, half, p).start()
+
+    lax.fori_loop(0, 4, functools.partial(first, 0), 0)
+    quad_logs()
+    lax.fori_loop(0, 4, functools.partial(first, 1), 0)
+    z_logs()
+    combine(0)
+    z_send(0, 0)
+    lax.fori_loop(0, 4, functools.partial(first, 2), 0)
+    lax.fori_loop(0, 1, inner, 0)
+    z_recv(0, 0)
+    for r in range(1, rounds):
+        z_send(r, 0)
+        if r < rounds - 1:
+            z_recv(r, 0)
+    combine(1)
+    z_send(0, 1)
+    lax.fori_loop(1, 2, inner, 0)
+    z_recv(0, 1)
+    for r in range(1, rounds):
+        z_send(r, 1)
+        if r < rounds - 1:
+            z_recv(r, 1)
+    combine(2)
+    z_send(0, 2)
+    if rounds > 1:
+        z_recv(rounds - 1, 0)
+    down(0)
+    lax.fori_loop(2, 3, inner, 0)
+    z_recv(0, 2)
+    for r in range(1, rounds):
+        z_send(r, 2)
+        if r < rounds - 1:
+            z_recv(r, 2)
+    if rounds > 1:
+        z_recv(rounds - 1, 1)
+    down(1)
+    lax.fori_loop(3, hp, inner, 0)
+    if rounds > 1:
+        z_recv(rounds - 1, 2)
+    down(2)
+    z_load.wait()
+    for k in range(3):
+        lax.fori_loop(0, 4, functools.partial(last, k), 0)
+        if k > 0:
+            finish(k - 1)
+    finish(2)
+
+    for x in range(2):
+
+        @pl.when(x * 2 + holder != here)
+        def _(x=x):
+            for i in range(5):
+                param_copy(i, x).wait_send()
+
+    for low, sends in ((True, sends_low), (False, sends_high)):
+
+        @pl.when(sends)
+        def _(low=low):
+            for i in range(3):
+                for k in range(2):
+                    edge_copy(i, low, k).wait_send()
+
+    for i in range(3):
+        inc_copy(i).wait_send()
+        half_copy(i).wait_send()
+        qlog_copy(i).wait_send()
+    for o in range(1, nz):
+        zlog_copy(o).wait_send()
+    for k in range(3):
+        for i in range(3):
+            up_copy(k, i).wait_send()
+            down_copy(k, i).wait_send()
+        for p in range(hp):
+            mix_copy(k, p).wait_send()
+        for r in range(rounds):
+            h, _, senders = z_parts(r)
+            for d, sender in senders:
+
+                @pl.when(sender)
+                def _(k=k, r=r, d=d, h=h):
+                    for o in range(1, h + 1):
+                        z_copy(r, k, o, d).wait_send()
+
+    for k in range(3):
+        for half in range(2):
+            for p in range(hp):
+                out_copy(k, half, p).wait()
+
+
+def fits_quad(sp, dp, blk, heads, groups):
+    nz = dp // 2
+    power = dp % 2 == 0 and nz > 1 and nz & (nz - 1) == 0
+    shares = sp == 4 and groups % 4 == 0 and groups // 4 == sp
+    return power and shares and blk == 128 and 2 * heads * HEAD_DIM == 3 * groups * 128
+
+
+def quad_local(sp, dp, x, b, c, z, ahead, back, spike, wx, wb, wc, offset, fading, gain):
+    x, b, c, z = x[0], b[0], c[0], z[0]
+    blk, x_total = x.shape
+    b_total = b.shape[1]
+    groups = b_total // STATE
+    heads = ahead.shape[2]
+    pairs = groups // 2
+    nz = dp // 2
+    rounds = nz.bit_length() - 1
+    tiles = heads // pairs * HEAD_DIM // 128
+    hp, hh = pairs // 2, heads // 2
+    x_half, b_half = x_total // 2, b_total // 2
+    width = x_half + 2 * b_half
+    params = (wx, wb, wc, offset, fading)
+    vm = pltpu.VMEM
+    gains = gain.reshape(x_total // 128, 128)
+    scratch = [vm(one.shape, BF16) for one in (x, b, c, z)]
+    scratch += [vm((2, 3, hh, blk), F32), vm((3, hh, blk), F32), vm(gains.shape, BF16)]
+    scratch += [vm((blk, x_half), BF16), vm((blk, b_half), BF16), vm((blk, b_half), BF16)]
+    scratch += [vm(one.shape, one.dtype) for one in params]
+    scratch += [vm((2,) + one.shape, one.dtype) for one in params]
+    scratch += [vm((EDGE, n), BF16) for n in (x_half, b_half, b_half)] * 2
+    scratch += [vm((2, 2 * blk + 16, 128), F32), vm((8, width), F32), vm((8, 128), F32)]
+    scratch += [vm((8, x_total), F32)] + [vm((2 * blk, 128), F32)] * 3
+    scratch += [vm((128, 2 * blk), F32)] * 3
+    scratch += [vm((2 * blk, x_half), BF16), vm((2 * hp, STATE, 2 * blk), BF16)]
+    scratch += [vm((2 * blk, b_half), BF16), vm((2 * blk, x_half), F32)]
+    scratch += [vm((tiles, 4, 2, STATE, 128), BF16)] * 4
+    scratch += [vm((8, 128), F32), vm((4, 8, 128), F32), vm((8, 128), F32), vm((nz, 8, 128), F32)]
+    scratch += [vm((4, 2, tiles, 8, 128), F32)] * 2 + [vm((2, tiles, 8, 128), F32)]
+    scratch += [vm((rounds, 2, tiles, 8, 128), F32)]
+    scratch += [vm((tiles, 2, STATE, 128), F32)] * 2 + [vm((rounds, tiles, STATE, 128), BF16)] * 2
+    scratch += [vm((tiles, hp, blk, 128), BF16)] * 2 + [vm((blk, x_total), BF16)]
+    dma = pltpu.SemaphoreType.DMA
+    scratch += [dma((16,)), dma((2, 5, 2)), dma((2, 3, 2)), dma((2, 3)), dma((2, 3))]
+    scratch += [dma((2, 4)), dma((2, nz)), dma((2, tiles, 4)), dma((rounds, tiles, nz))]
+    scratch += [dma((rounds, tiles)), dma((2, tiles, 4)), dma((2, tiles, hp)), dma((tiles, 2, hp))]
+    out = pl.pallas_call(
+        functools.partial(quad_kernel, (heads, pairs, sp, dp)),
+        out_shape=jax.ShapeDtypeStruct((blk, x_total), BF16),
+        in_specs=[pl.BlockSpec(memory_space=pl.ANY)] * 13,
+        out_specs=pl.BlockSpec(memory_space=pl.ANY),
+        scratch_shapes=scratch,
+        compiler_params=pltpu.CompilerParams(
+            collective_id=0, has_side_effects=True, vmem_limit_bytes=40 * 2**20
+        ),
+        name="mixer",
+    )(x, b, c, z, ahead[0].T, back[0].T, spike[0].T, *params, gains)
+    return out[None]
+
+
+def pick(sp, dp, x, b, *rest):
+    blk, heads = x.shape[1], rest[2].shape[2]
+    if fits_quad(sp, dp, blk, heads, b.shape[2] // STATE):
+        return quad_local(sp, dp, x, b, *rest)
+    return local(sp, dp, x, b, *rest)
+
+
 def solution(mesh):
     tokens = P("dp", "sp", None)
     placed = (tokens,) * 7 + (P(None, "sp"),) * 5 + (P(),)
     return jax.shard_map(
-        functools.partial(local, mesh.shape["sp"], mesh.shape["dp"]),
+        functools.partial(pick, mesh.shape["sp"], mesh.shape["dp"]),
         mesh=mesh,
         in_specs=placed,
         out_specs=tokens,

time: 62.1 us -> 49.6 us (0.80)
  the two profiles are of different devices: /device:TPU:8 before, /device:TPU:0 now
where the time goes in v1:
time: 49.6 us; the launch traced here: 49 us
  Pallas kernels  39.5 us (80%)
  local copies, waits for them, and re-layouts  9.54 us (19%)
    pallas_call x1, Pallas kernels, quad_local(): pl.pallas_call(functools.partial(quad_kernel, (heads, pairs, sp, dp)), ou...  39.5 us
    unnamed x27, local copies, waits for them, and re-layouts  9.54 us

profile of v1, /device:TPU:0, one launch (start us, length us, event | category | flops | bytes accessed | tf_op | source)
XLA Modules:
  0.0 49.0 jit_solution(8472845266141318332)
XLA Ops:
  0.0 0.0 copy-start.12
  0.0 0.0 copy-start.8
  0.0 0.0 copy-start.7
  0.0 0.0 copy-start.11
  0.0 0.7 %copy-done.12 = f32[2,12]{1,0:T(2,128)S(1)} copy-done((f32[2,12]{1,0:T(2,128)S(1)}, f32[2,12]{1,0:T(2,128)}, u32[]{:S(2)}) %copy-start.12) | copy-done | bytes 120
  0.7 0.0 copy-done.8
  0.7 0.0 copy-done.7
  0.7 0.0 copy-done.11
  0.7 0.0 copy-start
  0.7 1.1 %copy-done = bf16[1,128,3072]{2,1,0:T(8,128)(2,1)S(1)} copy-done((bf16[1,128,3072]{2,1,0:T(8,128)(2,1)S(1)}, bf16[1,128,3072]{2,1,0:T(8,128)(2,1)}, u32[]{:S(2)}) %copy-start) | copy-done | bytes 786456
  1.9 0.0 copy-start.1
  1.9 1.1 %copy-done.1 = bf16[1,128,3072]{2,1,0:T(8,128)(2,1)S(1)} copy-done((bf16[1,128,3072]{2,1,0:T(8,128)(2,1)S(1)}, bf16[1,128,3072]{2,1,0:T(8,128)(2,1)}, u32[]{:S(2)}) %copy-start.1) | copy-done | bytes 786456
  3.0 0.0 copy-start.2
  3.0 1.0 %copy-done.2 = bf16[1,128,2048]{2,1,0:T(8,128)(2,1)S(1)} copy-done((bf16[1,128,2048]{2,1,0:T(8,128)(2,1)S(1)}, bf16[1,128,2048]{2,1,0:T(8,128)(2,1)}, u32[]{:S(2)}) %copy-start.2) | copy-done | bytes 524312
  4.0 0.0 copy-start.3
  4.0 1.0 %copy-done.3 = bf16[1,128,2048]{2,1,0:T(8,128)(2,1)S(1)} copy-done((bf16[1,128,2048]{2,1,0:T(8,128)(2,1)S(1)}, bf16[1,128,2048]{2,1,0:T(8,128)(2,1)}, u32[]{:S(2)}) %copy-start.3) | copy-done | bytes 524312
  5.1 0.0 copy-start.4
  5.1 0.7 %copy-done.4 = f32[1,128,48]{1,2,0:T(8,128)S(1)} copy-done((f32[1,128,48]{1,2,0:T(8,128)S(1)}, f32[1,128,48]{1,2,0:T(8,128)}, u32[]{:S(2)}) %copy-start.4) | copy-done | bytes 24600
  5.8 0.0 copy-start.5
  5.8 0.7 %copy-done.5 = f32[1,128,48]{1,2,0:T(8,128)S(1)} copy-done((f32[1,128,48]{1,2,0:T(8,128)S(1)}, f32[1,128,48]{1,2,0:T(8,128)}, u32[]{:S(2)}) %copy-start.5) | copy-done | bytes 24600
  6.6 0.0 copy-start.6
  6.6 0.7 %copy-done.6 = f32[1,128,48]{1,2,0:T(8,128)S(1)} copy-done((f32[1,128,48]{1,2,0:T(8,128)S(1)}, f32[1,128,48]{1,2,0:T(8,128)}, u32[]{:S(2)}) %copy-start.6) | copy-done | bytes 24600
  7.3 0.0 copy-start.9
  7.3 0.7 %copy-done.9 = bf16[4,512]{1,0:T(4,128)(2,1)S(1)} copy-done((bf16[4,512]{1,0:T(4,128)(2,1)S(1)}, bf16[4,512]{1,0:T(4,128)(2,1)}, u32[]{:S(2)}) %copy-start.9) | copy-done | bytes 4120
  8.0 0.0 copy-start.10
  8.0 0.7 %copy-done.10 = bf16[4,512]{1,0:T(4,128)(2,1)S(1)} copy-done((bf16[4,512]{1,0:T(4,128)(2,1)S(1)}, bf16[4,512]{1,0:T(4,128)(2,1)}, u32[]{:S(2)}) %copy-start.10) | copy-done | bytes 4120
  8.7 39.5 %mixer.1 = bf16[128,3072]{1,0:T(8,128)(2,1)S(1)} custom-call(bf16[128,3072]{1,0:T(8,128)(2,1)S(1)} %bitcast.16, bf16[128,2048]{1,0:T(8,128)(2,1)S(1)} %bitcast.18, bf16[128,2048]{1,0:T(8,128)(2,1)S(1)} %bitcast.19, bf16[128,3072]{1,0:T(8,128)(2,1)S(1)} %bitcast.17, f32[48,128]{1,0:T(8,128)S(1)} %bitcast.20, f32[48,128]{1,0:T(8,128)S(1)} %bitcast.21, ...), custom_call_target="tpu_custom_call" | custom-call | tf_op jit(solution)/shard_map/mixer/pallas_call | solution.py:1238
  48.1 0.9 %copy.15 = bf16[1,128,3072]{2,1,0:T(8,128)(2,1)} copy(bf16[1,128,3072]{2,1,0:T(8,128)(2,1)S(1)} %bitcast.15) | data formatting | bytes 1572864
Async XLA Ops:
  0.0 0.7 %copy-start.12 = (f32[2,12]{1,0:T(2,128)S(1)}, f32[2,12]{1,0:T(2,128)}, u32[]{:S(2)}) copy-start(f32[2,12]{1,0:T(2,128)} %refs_11_.1) | copy-start | bytes 292
  0.0 0.7 %copy-start.8 = (bf16[3072]{0:T(1024)(128)(2,1)S(1)}, bf16[3072]{0:T(1024)(128)(2,1)}, u32[]{:S(2)}) copy-start(bf16[3072]{0:T(1024)(128)(2,1)} %param.25) | copy-start | bytes 18436
  0.0 0.7 %copy-start.7 = (bf16[4,768]{1,0:T(4,128)(2,1)S(1)}, bf16[4,768]{1,0:T(4,128)(2,1)}, u32[]{:S(2)}) copy-start(bf16[4,768]{1,0:T(4,128)(2,1)} %refs_7_.1) | copy-start | bytes 18436
  0.0 0.7 %copy-start.11 = (f32[2,12]{1,0:T(2,128)S(1)}, f32[2,12]{1,0:T(2,128)}, u32[]{:S(2)}) copy-start(f32[2,12]{1,0:T(2,128)} %refs_10_.1) | copy-start | bytes 292
  0.7 1.1 %copy-start = (bf16[1,128,3072]{2,1,0:T(8,128)(2,1)S(1)}, bf16[1,128,3072]{2,1,0:T(8,128)(2,1)}, u32[]{:S(2)}) copy-start(bf16[1,128,3072]{2,1,0:T(8,128)(2,1)} %param.13) | copy-start | bytes 2359300
  1.9 1.1 %copy-start.1 = (bf16[1,128,3072]{2,1,0:T(8,128)(2,1)S(1)}, bf16[1,128,3072]{2,1,0:T(8,128)(2,1)}, u32[]{:S(2)}) copy-start(bf16[1,128,3072]{2,1,0:T(8,128)(2,1)} %param.16) | copy-start | bytes 2359300
  3.0 1.0 %copy-start.2 = (bf16[1,128,2048]{2,1,0:T(8,128)(2,1)S(1)}, bf16[1,128,2048]{2,1,0:T(8,128)(2,1)}, u32[]{:S(2)}) copy-start(bf16[1,128,2048]{2,1,0:T(8,128)(2,1)} %param.14) | copy-start | bytes 1572868
  4.0 1.0 %copy-start.3 = (bf16[1,128,2048]{2,1,0:T(8,128)(2,1)S(1)}, bf16[1,128,2048]{2,1,0:T(8,128)(2,1)}, u32[]{:S(2)}) copy-start(bf16[1,128,2048]{2,1,0:T(8,128)(2,1)} %param.15) | copy-start | bytes 1572868
  5.1 0.7 %copy-start.4 = (f32[1,128,48]{1,2,0:T(8,128)S(1)}, f32[1,128,48]{1,2,0:T(8,128)}, u32[]{:S(2)}) copy-start(f32[1,128,48]{1,2,0:T(8,128)} %param.17) | copy-start | bytes 73732
  5.8 0.7 %copy-start.5 = (f32[1,128,48]{1,2,0:T(8,128)S(1)}, f32[1,128,48]{1,2,0:T(8,128)}, u32[]{:S(2)}) copy-start(f32[1,128,48]{1,2,0:T(8,128)} %param.18) | copy-start | bytes 73732
  6.6 0.7 %copy-start.6 = (f32[1,128,48]{1,2,0:T(8,128)S(1)}, f32[1,128,48]{1,2,0:T(8,128)}, u32[]{:S(2)}) copy-start(f32[1,128,48]{1,2,0:T(8,128)} %param.19) | copy-start | bytes 73732
  7.3 0.7 %copy-start.9 = (bf16[4,512]{1,0:T(4,128)(2,1)S(1)}, bf16[4,512]{1,0:T(4,128)(2,1)}, u32[]{:S(2)}) copy-start(bf16[4,512]{1,0:T(4,128)(2,1)} %refs_8_.1) | copy-start | bytes 12292
  8.0 0.7 %copy-start.10 = (bf16[4,512]{1,0:T(4,128)(2,1)S(1)}, bf16[4,512]{1,0:T(4,128)(2,1)}, u32[]{:S(2)}) copy-start(bf16[4,512]{1,0:T(4,128)(2,1)} %refs_9_.1) | copy-start | bytes 12292

commit v2 on v1

--- a/solution.py
+++ b/solution.py
@@ -565,16 +565,16 @@
     rounds = nz.bit_length() - 1
     (x_hbm, b_hbm, c_hbm, z_hbm, ahead_hbm, back_hbm, spike_hbm) = refs[:7]
     params = refs[7:12]
-    gain_hbm, out_hbm = refs[12:14]
+    gain_hbm, out_ref = refs[12:14]
     (in_x, in_b, in_c, in_z, inc, inc_out, gain_in, px, pb, pc) = refs[14:24]
     own, got = refs[24:29], refs[29:34]
     edges = refs[34:40]
     (work, w_ref, prm_ref, gain_ref, cum_ref, fac_ref, col_ref, cum_t, rate_t, mid_t) = refs[40:50]
     (xc, bt, cc, y_ref, sup, up_in, down_out, down_in) = refs[50:58]
     (logs, qlog, zsum, zlog, dec, wup, zdec, zwt) = refs[58:66]
-    (tz, zin, zs, zr, mix_out, mix_in, out_v) = refs[66:73]
-    (load_sem, prm_sem, edge_sem, half_sem, inc_sem, qlog_sem, zlog_sem) = refs[73:80]
-    (up_sem, zsend_sem, zrecv_sem, down_sem, mix_sem, out_sem) = refs[80:86]
+    (tz, zin, zs, zr, mix_out, mix_in) = refs[66:72]
+    (load_sem, prm_sem, edge_sem, half_sem, inc_sem, qlog_sem, zlog_sem) = refs[72:79]
+    (up_sem, zsend_sem, zrecv_sem, down_sem, mix_sem) = refs[79:84]
 
     hh = heads // 2
     hp = pairs // 2
@@ -1050,7 +1050,7 @@
         low = jnp.sum(jnp.where(left, square, 0.0), axis=1, keepdims=True)
         high = jnp.sum(jnp.where(left, 0.0, square), axis=1, keepdims=True)
         mean = jnp.where(left, low, high) * (1.0 / HEAD_DIM)
-        out_v[:, at] = (gated * lax.rsqrt(mean + 1e-6) * gain_ref[0:1, at]).astype(BF16)
+        out_ref[:, at] = (gated * lax.rsqrt(mean + 1e-6) * gain_ref[0:1, at]).astype(BF16)
 
     def mix_copy(k, p):
         return remote(
@@ -1088,10 +1088,6 @@
                 mix_copy(k, p).start()
         return 0
 
-    def out_copy(k, half, p):
-        at = pl.ds(pl.multiple_of(half * x_half + p * x_w + k * 128, 128), 128)
-        return pltpu.make_async_copy(out_v.at[:, at], out_hbm.at[:, at], out_sem.at[k, half, p])
-
     def take(k, p, _):
         mix_copy(k, p).wait_recv()
         gate(mix_in[k, p], pl.ds(pl.multiple_of(other * x_half + p * x_w + k * 128, 128), 128))
@@ -1099,9 +1095,6 @@
 
     def finish(k):
         lax.fori_loop(0, hp, functools.partial(take, k), 0)
-        for half in range(2):
-            for p in range(hp):
-                out_copy(k, half, p).start()
 
     lax.fori_loop(0, 4, functools.partial(first, 0), 0)
     quad_logs()
@@ -1185,11 +1178,6 @@
                     for o in range(1, h + 1):
                         z_copy(r, k, o, d).wait_send()
 
-    for k in range(3):
-        for half in range(2):
-            for p in range(hp):
-                out_copy(k, half, p).wait()
-
 
 def fits_quad(sp, dp, blk, heads, groups):
     nz = dp // 2
@@ -1230,19 +1218,19 @@
     scratch += [vm((4, 2, tiles, 8, 128), F32)] * 2 + [vm((2, tiles, 8, 128), F32)]
     scratch += [vm((rounds, 2, tiles, 8, 128), F32)]
     scratch += [vm((tiles, 2, STATE, 128), F32)] * 2 + [vm((rounds, tiles, STATE, 128), BF16)] * 2
-    scratch += [vm((tiles, hp, blk, 128), BF16)] * 2 + [vm((blk, x_total), BF16)]
+    scratch += [vm((tiles, hp, blk, 128), BF16)] * 2
     dma = pltpu.SemaphoreType.DMA
     scratch += [dma((16,)), dma((2, 5, 2)), dma((2, 3, 2)), dma((2, 3)), dma((2, 3))]
     scratch += [dma((2, 4)), dma((2, nz)), dma((2, tiles, 4)), dma((rounds, tiles, nz))]
-    scratch += [dma((rounds, tiles)), dma((2, tiles, 4)), dma((2, tiles, hp)), dma((tiles, 2, hp))]
+    scratch += [dma((rounds, tiles)), dma((2, tiles, 4)), dma((2, tiles, hp))]
     out = pl.pallas_call(
         functools.partial(quad_kernel, (heads, pairs, sp, dp)),
-        out_shape=jax.ShapeDtypeStruct((blk, x_total), BF16),
-        in_specs=[pl.BlockSpec(memory_space=pl.ANY)] * 13,
-        out_specs=pl.BlockSpec(memory_space=pl.ANY),
+        out_shape=pltpu.VMEM((blk, x_total), BF16),
+        in_specs=[pl.BlockSpec(memory_space=pltpu.HBM)] * 13,
+        out_specs=pl.BlockSpec(memory_space=pltpu.VMEM),
         scratch_shapes=scratch,
         compiler_params=pltpu.CompilerParams(
-            collective_id=0, has_side_effects=True, vmem_limit_bytes=40 * 2**20
+            collective_id=0, has_side_effects=True, vmem_limit_bytes=60 * 2**20
         ),
         name="mixer",
     )(x, b, c, z, ahead[0].T, back[0].T, spike[0].T, *params, gains)

time: 49.6 us -> 40.1 us (0.81)
  local copies, waits for them, and re-layouts: 9.54 us -> 0.88 us
  Pallas kernels: 39.5 us -> 39 us
    unnamed x27 -> x1, local copies, waits for them, and re-layouts: 9.54 us -> 0.88 us
where the time goes in v2:
time: 40.1 us; the launch traced here: 39.9 us
  Pallas kernels  39 us (97%)
  local copies, waits for them, and re-layouts  0.88 us (2%)
    pallas_call x1, Pallas kernels, quad_local(): pl.pallas_call(functools.partial(quad_kernel, (heads, pairs, sp, dp)), ou...  39 us
    unnamed x1, local copies, waits for them, and re-layouts  0.88 us

profile of v2, /device:TPU:0, one launch (start us, length us, event | category | flops | bytes accessed | tf_op | source)
XLA Modules:
  0.0 39.9 jit_solution(8229641059524979450)
XLA Ops:
  0.0 39.0 %mixer.1 = bf16[128,3072]{1,0:T(8,128)(2,1)S(1)} custom-call(bf16[128,3072]{1,0:T(8,128)(2,1)} %bitcast.16, bf16[128,2048]{1,0:T(8,128)(2,1)} %bitcast.18, bf16[128,2048]{1,0:T(8,128)(2,1)} %bitcast.19, bf16[128,3072]{1,0:T(8,128)(2,1)} %bitcast.17, f32[48,128]{1,0:T(8,128)} %bitcast.20, f32[48,128]{1,0:T(8,128)} %bitcast.21, f32[48,128]{1,0:T(8,128)} %bitcast.22, ...), custom_call_target="tpu_custom_call" | custom-call | tf_op jit(solution)/shard_map/mixer/pallas_call | solution.py:1226
  39.0 0.9 %copy.15 = bf16[1,128,3072]{2,1,0:T(8,128)(2,1)} copy(bf16[1,128,3072]{2,1,0:T(8,128)(2,1)S(1)} %bitcast.15) | data formatting | bytes 1572864

commit v3 on v2

--- a/solution.py
+++ b/solution.py
@@ -570,6 +570,8 @@
     own, got = refs[24:29], refs[29:34]
     edges = refs[34:40]
     (work, w_ref, prm_ref, gain_ref, cum_ref, fac_ref, col_ref, cum_t, rate_t, mid_t) = refs[40:50]
+    low_ref, high_ref, bc, zg = refs[50:54]
+    refs = refs[:50] + refs[54:]
     (xc, bt, cc, y_ref, sup, up_in, down_out, down_in) = refs[50:58]
     (logs, qlog, zsum, zlog, dec, wup, zdec, zwt) = refs[58:66]
     (tz, zin, zs, zr, mix_out, mix_in) = refs[66:72]
@@ -764,8 +766,10 @@
         off = 0
         for i in range(3):
             n = own[i].shape[1]
-            w_ref[0:4, off + q * n : off + (q + 1) * n] = got[i][q].astype(F32)
-            off += 2 * n
+            part = got[i][q].astype(F32)
+            for t in range(n // 128):
+                w_ref[off + q * (n // 128) + t, 0:4, :] = part[:, t * 128 : (t + 1) * 128]
+            off += 2 * n // 128
 
     cums, rates = [], []
     for j in range(2):
@@ -806,21 +810,12 @@
         mid = rates[j] * jnp.exp(jnp.minimum((mid_f if j == 0 else mid_b) - near, 0.0))
         mid_t[:, at] = mid.T
 
-    for k in range(gain_in.shape[0]):
-        if k == 0:
-            gain_load.wait()
-        gain_ref[0:1, k * 128 : (k + 1) * 128] = gain_in[k : k + 1, :].astype(F32)
+    gain_load.wait()
+    gain_ref[...] = gain_in[...].astype(F32)
 
     for i in range(3):
         remote(sources[i].at[:, pl.ds(0, halves[i])], (px, pb, pc)[i], half_sem.at[0, i],
                half_sem.at[1, i], partner).wait_recv()
-    for low, present in ((True, has_prev), (False, has_next)):
-
-        @pl.when(present)
-        def _(low=low):
-            for i in range(3):
-                edge_copy(i, low, 0).wait_recv()
-
     def rolled(v, p):
         return pltpu.roll(v, lax.rem(128 - p * per_pair, 128), 1)
 
@@ -828,24 +823,67 @@
         mask = lax.broadcasted_iota(jnp.int32, (cols.shape[0], 128), 1) < HEAD_DIM
         return jnp.where(mask, cols[:, i : i + 1], cols[:, i + 1 : i + 2])
 
-    offsets = (0, 2 * own[0].shape[1], 2 * own[0].shape[1] + 2 * own[1].shape[1])
-
-    def conv(i, col, spot):
-        half = halves[i]
-        mine_at = pl.ds(pl.multiple_of(core * half + col, 128), 128)
-        at = pl.ds(pl.multiple_of(col, 128), 128)
-        buf = work.at[spot]
-        buf[pl.ds(pl.multiple_of(8 + core * blk, 8), blk), :] = sources[i][:, mine_at].astype(F32)
-        buf[pl.ds(pl.multiple_of(8 + other * blk, 8), blk), :] = (px, pb, pc)[i][:, at].astype(F32)
-        buf[0:8, :] = jnp.where(has_prev, edges[i][:, at].astype(F32), 0.0)
-        high = jnp.where(has_next, edges[3 + i][:, at].astype(F32), 0.0)
-        buf[8 + tokens : 16 + tokens, :] = high
-        w_at = pl.ds(pl.multiple_of(offsets[i] + col, 128), 128)
-        s = buf[6 : 6 + tokens, :] * w_ref[0:1, w_at]
-        for k in range(1, 4):
-            s = s + buf[6 + k : 6 + k + tokens, :] * w_ref[k : k + 1, w_at]
+    tiles_of = [half // 128 for half in halves]
+    starts = (0, tiles_of[0], tiles_of[0] + tiles_of[1])
+
+    def silu(s):
         h = 0.5 * s
         return h + h * jnp.tanh(h)
+
+    def store(i, t, rows, v):
+        if i == 1:
+            bc[t, rows, :] = v
+        else:
+            (xc, None, cc)[i][t, rows, :] = v.astype(BF16)
+
+    def conv(i, group, _):
+        for spot in range(4):
+            t = group * 4 + spot
+            mine_at = pl.ds(pl.multiple_of(core * halves[i] + t * 128, 128), 128)
+            at = pl.ds(pl.multiple_of(t * 128, 128), 128)
+            buf = work.at[spot]
+            here_at = pl.ds(pl.multiple_of(8 + core * blk, 8), blk)
+            there_at = pl.ds(pl.multiple_of(8 + other * blk, 8), blk)
+            buf[here_at, :] = sources[i][:, mine_at].astype(F32)
+            buf[there_at, :] = (px, pb, pc)[i][:, at].astype(F32)
+            s = buf[6 : 6 + tokens, :] * w_ref[starts[i] + t, 0:1, :]
+            for k in range(1, 4):
+                s = s + buf[6 + k : 6 + k + tokens, :] * w_ref[starts[i] + t, k : k + 1, :]
+            store(i, t, slice(0, tokens), silu(s))
+        return 0
+
+    def edge_wait(i):
+        for low, present in ((True, has_prev), (False, has_next)):
+
+            @pl.when(present)
+            def _(low=low):
+                edge_copy(i, low, 0).wait_recv()
+
+    def fix(i):
+        half = halves[i]
+        row16 = row[0:16]
+        own_part = sources[i]
+        their_part = (px, pb, pc)[i]
+        for t in range(tiles_of[i]):
+            mine_at = pl.ds(pl.multiple_of(core * half + t * 128, 128), 128)
+            at = slice(t * 128, (t + 1) * 128)
+            start = jnp.where(core == 0, own_part[0:8, mine_at], their_part[0:8, at])
+            end = jnp.where(core == 1, own_part[blk - 8 :, mine_at], their_part[blk - 8 :, at])
+            low_ref[t, 0:8, :] = jnp.where(has_prev, edges[i][:, at].astype(F32), 0.0)
+            low_ref[t, 8:16, :] = start.astype(F32)
+            high_ref[t, 8:16, :] = end.astype(F32)
+            high_ref[t, 16:24, :] = jnp.where(has_next, edges[3 + i][:, at].astype(F32), 0.0)
+        dst = (xc, bc, cc)[i]
+        for t in range(tiles_of[i]):
+            for ref, low in ((low_ref, True), (high_ref, False)):
+                s = ref[t, 6:14, :] * w_ref[starts[i] + t, 0:1, :]
+                for k in range(1, 4):
+                    s = s + ref[t, 6 + k : 14 + k, :] * w_ref[starts[i] + t, k : k + 1, :]
+                s = silu(s)
+                rows = slice(0, 16) if low else slice(tokens - 16, tokens)
+                s = jnp.concatenate([s, s], axis=0)
+                keep = row16 >= 2 if low else row16 < 15
+                store(i, t, rows, jnp.where(keep, dst[t, rows, :].astype(F32), s))
 
     def up_copy(k, i):
         qy, qx, q = member(i)
@@ -857,43 +895,28 @@
     def wide_left(n):
         return lax.rem(lax.broadcasted_iota(jnp.int32, (128, n), 1), 128) < HEAD_DIM
 
-    def first(k, i, _):
-        _, _, p = member(i)
-        if k < 2:
-            g = 2 * p + k
-            bt[g] = conv(1, g * 128, 0).T.astype(BF16)
-        col = p * x_w + k * 128
-        xv = conv(0, col, 1).astype(BF16)
-        xc[:, pl.ds(pl.multiple_of(col, 128), 128)] = xv
-        xf = xv.astype(F32)
-        cols = rolled(fac_ref[...], p)
-        rhs = jnp.concatenate(
-            [(xf * two(cols, d * hh + 2 * k)).astype(BF16) for d in range(2)], axis=1
-        )
-        u = jnp.dot(bt[2 * p + k // 2], rhs, preferred_element_type=F32)
-        if k == 1:
-            v = jnp.dot(bt[2 * p + 1], rhs, preferred_element_type=F32)
-            u = jnp.where(wide_left(256), u, v)
-        u = u.astype(BF16)
-
-        @pl.when(i < 3)
-        def _():
+    def first(k):
+        fac = fac_ref[...]
+        for p in range(hp):
+            if k < 2:
+                bt[2 * p + k] = bc[2 * p + k].T.astype(BF16)
+            xf = xc[p * tiles + k].astype(F32)
+            head = p * per_pair + 2 * k
+            rhs = jnp.concatenate(
+                [(xf * two(fac, d * hh + head)).astype(BF16) for d in range(2)], axis=1
+            )
+            u = jnp.dot(bt[2 * p + k // 2], rhs, preferred_element_type=F32)
+            if k == 1:
+                v = jnp.dot(bt[2 * p + 1], rhs, preferred_element_type=F32)
+                u = jnp.where(wide_left(256), u, v)
+            u = u.astype(BF16)
             sup[k, p, 0] = u[:, :128]
             sup[k, p, 1] = u[:, 128:]
+        for i in range(3):
             up_copy(k, i).start()
-
-        @pl.when(i == 3)
-        def _():
-            up_in[k, p, 0] = u[:, :128]
-            up_in[k, p, 1] = u[:, 128:]
-
-        return 0
+        up_in[k, me] = sup[k, me]
 
     def inner(p, _):
-        x_at = [pl.ds(pl.multiple_of(p * x_w + k * 128, 128), 128) for k in range(tiles)]
-        for g in range(2):
-            at = pl.ds(pl.multiple_of((2 * p + g) * 128, 128), 128)
-            cc[:, at] = conv(2, (2 * p + g) * 128, g).astype(BF16)
         for r in range(2):
             rows = slice(r * blk, (r + 1) * blk)
             cols = rolled(col_ref[rows, :], p)
@@ -901,8 +924,7 @@
             shift = rolled(jnp.exp(jnp.minimum(col_ref[rows, :] - mid_row, 0.0)), p)
             parts = []
             for g in range(2):
-                at = pl.ds(pl.multiple_of((2 * p + g) * 128, 128), 128)
-                scores = jnp.dot(cc[rows, at], bt[2 * p + g], preferred_element_type=F32)
+                scores = jnp.dot(cc[2 * p + g, rows], bt[2 * p + g], preferred_element_type=F32)
                 on = scores[:, r * blk : (r + 1) * blk]
                 away = scores[:, (1 - r) * blk : (2 - r) * blk]
                 for h in range(g * per_pair // 2, (g + 1) * per_pair // 2):
@@ -921,14 +943,14 @@
                     far = (away * shift[:, c : c + 1] * far_row).astype(BF16)
                     parts.append(jnp.concatenate([near, far] if r == 0 else [far, near], axis=1))
             for k in range(tiles):
-                xt = xc[:, x_at[k]]
+                xt = xc[p * tiles + k]
                 zero = jnp.zeros_like(xt)
                 mask = lax.broadcasted_iota(jnp.int32, xt.shape, 1) < HEAD_DIM
                 both = jnp.concatenate(
                     [jnp.where(mask, xt, zero), jnp.where(mask, zero, xt)], axis=0
                 )
                 w = jnp.concatenate([parts[2 * k], parts[2 * k + 1]], axis=1)
-                y_ref[rows, x_at[k]] = jnp.dot(w, both, preferred_element_type=F32)
+                y_ref[p * tiles + k, rows] = jnp.dot(w, both, preferred_element_type=F32)
         return 0
 
     def zlog_copy(o):
@@ -1042,67 +1064,80 @@
             down_copy(k, i).start()
         down_in[k, me] = down_out[k, me]
 
-    def gate(mixed, at):
-        z = in_z[:, at].astype(F32)
-        half_z = 0.5 * z
-        gated = mixed.astype(F32) * (half_z + half_z * jnp.tanh(half_z))
+    def gates(group, _):
+        for spot in range(4):
+            t = group * 4 + spot
+            z = in_z[:, pl.ds(pl.multiple_of(t * 128, 128), 128)].astype(F32)
+            zg[t] = silu(z)
+        return 0
+
+    def gate(mixed, t):
+        gated = mixed.astype(F32) * zg[t]
         square = gated * gated
         low = jnp.sum(jnp.where(left, square, 0.0), axis=1, keepdims=True)
         high = jnp.sum(jnp.where(left, 0.0, square), axis=1, keepdims=True)
         mean = jnp.where(left, low, high) * (1.0 / HEAD_DIM)
-        out_ref[:, at] = (gated * lax.rsqrt(mean + 1e-6) * gain_ref[0:1, at]).astype(BF16)
-
-    def mix_copy(k, p):
+        scale = lax.rsqrt(mean + 1e-6) * gain_ref[pl.ds(t, 1), :]
+        out_ref[:, pl.ds(pl.multiple_of(t * 128, 128), 128)] = (gated * scale).astype(BF16)
+
+    def mix_copy(k):
         return remote(
-            mix_out.at[k, p], mix_in.at[k, p], mix_sem.at[0, k, p], mix_sem.at[1, k, p], partner
-        )
-
-    def last(k, j, _):
-        i = 3 - j
-        _, _, p = member(i)
-
-        @pl.when(i < 3)
-        def _():
+            mix_out.at[k], mix_in.at[k], mix_sem.at[0, k], mix_sem.at[1, k], partner
+        )
+
+    def last(k):
+        for i in range(3):
+            _, _, q = member(i)
             remote(
-                down_out.at[k, p], down_in.at[k, p], down_sem.at[0, k, i], down_sem.at[1, k, p],
+                down_out.at[k, q], down_in.at[k, q], down_sem.at[0, k, i], down_sem.at[1, k, q],
                 partner,
             ).wait_recv()
-
-        rhs = jnp.concatenate([down_in[k, p, 0], down_in[k, p, 1]], axis=1)
-        at = pl.ds(pl.multiple_of(p * x_w + k * 128, 128), 128)
         for mine in (False, True):
-            start = pl.multiple_of((core if mine else other) * blk, 128)
-            rows = pl.ds(start, blk)
-            c_at = [pl.ds(pl.multiple_of((2 * p + g) * 128, 128), 128) for g in range(2)]
-            v = jnp.dot(cc[rows, c_at[k // 2]], rhs, preferred_element_type=F32)
-            if k == 1:
-                u = jnp.dot(cc[rows, c_at[1]], rhs, preferred_element_type=F32)
-                v = jnp.where(wide_left(256), v, u)
-            cols = rolled(cum_ref[rows, :], p)
-            y = y_ref[rows, at] + v[:, :128] * two(cols, 2 * k) + v[:, 128:] * two(cols, hh + 2 * k)
-            mixed = y.astype(BF16)
-            if mine:
-                gate(mixed, pl.ds(pl.multiple_of(core * x_half + p * x_w + k * 128, 128), 128))
-            else:
-                mix_out[k, p] = mixed
-                mix_copy(k, p).start()
-        return 0
-
-    def take(k, p, _):
-        mix_copy(k, p).wait_recv()
-        gate(mix_in[k, p], pl.ds(pl.multiple_of(other * x_half + p * x_w + k * 128, 128), 128))
-        return 0
+            rows = pl.ds(pl.multiple_of((core if mine else other) * blk, 128), blk)
+            cols = cum_ref[rows, :]
+            for p in range(hp):
+                rhs = jnp.concatenate([down_in[k, p, 0], down_in[k, p, 1]], axis=1)
+                v = jnp.dot(cc[2 * p + k // 2, rows], rhs, preferred_element_type=F32)
+                if k == 1:
+                    u = jnp.dot(cc[2 * p + 1, rows], rhs, preferred_element_type=F32)
+                    v = jnp.where(wide_left(256), v, u)
+                head = p * per_pair + 2 * k
+                t = p * tiles + k
+                y = y_ref[t, rows] + v[:, :128] * two(cols, head) + v[:, 128:] * two(cols, hh + head)
+                mixed = y.astype(BF16)
+                if mine:
+                    gate(mixed, core * tiles_of[0] + t)
+                else:
+                    mix_out[k, p] = mixed
+            if not mine:
+                mix_copy(k).start()
 
     def finish(k):
-        lax.fori_loop(0, hp, functools.partial(take, k), 0)
-
-    lax.fori_loop(0, 4, functools.partial(first, 0), 0)
+        mix_copy(k).wait_recv()
+        for p in range(hp):
+            gate(mix_in[k, p], other * tiles_of[0] + p * tiles + k)
+
+    for spot in range(4):
+        work[spot, 0:8, :] = jnp.zeros((8, 128), F32)
+        work[spot, 8 + tokens :, :] = jnp.zeros((8, 128), F32)
+    low_ref[...] = jnp.zeros_like(low_ref)
+    high_ref[...] = jnp.zeros_like(high_ref)
+    for i in (1, 0):
+        lax.fori_loop(0, tiles_of[i] // 4, functools.partial(conv, i), 0)
     quad_logs()
-    lax.fori_loop(0, 4, functools.partial(first, 1), 0)
+    for i in (1, 0):
+        edge_wait(i)
+    for i in (1, 0):
+        fix(i)
+    first(0)
+    first(1)
+    first(2)
+    lax.fori_loop(0, tiles_of[2] // 4, functools.partial(conv, 2), 0)
+    edge_wait(2)
+    fix(2)
     z_logs()
     combine(0)
     z_send(0, 0)
-    lax.fori_loop(0, 4, functools.partial(first, 2), 0)
     lax.fori_loop(0, 1, inner, 0)
     z_recv(0, 0)
     for r in range(1, rounds):
@@ -1136,8 +1171,9 @@
         z_recv(rounds - 1, 2)
     down(2)
     z_load.wait()
+    lax.fori_loop(0, 2 * tiles_of[0] // 4, gates, 0)
     for k in range(3):
-        lax.fori_loop(0, 4, functools.partial(last, k), 0)
+        last(k)
         if k > 0:
             finish(k - 1)
     finish(2)
@@ -1167,8 +1203,7 @@
         for i in range(3):
             up_copy(k, i).wait_send()
             down_copy(k, i).wait_send()
-        for p in range(hp):
-            mix_copy(k, p).wait_send()
+        mix_copy(k).wait_send()
         for r in range(rounds):
             h, _, senders = z_parts(r)
             for d, sender in senders:
@@ -1208,11 +1243,13 @@
     scratch += [vm(one.shape, one.dtype) for one in params]
     scratch += [vm((2,) + one.shape, one.dtype) for one in params]
     scratch += [vm((EDGE, n), BF16) for n in (x_half, b_half, b_half)] * 2
-    scratch += [vm((2, 2 * blk + 16, 128), F32), vm((8, width), F32), vm((8, 128), F32)]
-    scratch += [vm((8, x_total), F32)] + [vm((2 * blk, 128), F32)] * 3
+    scratch += [vm((4, 2 * blk + 16, 128), F32), vm((width // 128, 8, 128), F32)]
+    scratch += [vm((8, 128), F32), vm(gains.shape, F32)] + [vm((2 * blk, 128), F32)] * 3
     scratch += [vm((128, 2 * blk), F32)] * 3
-    scratch += [vm((2 * blk, x_half), BF16), vm((2 * hp, STATE, 2 * blk), BF16)]
-    scratch += [vm((2 * blk, b_half), BF16), vm((2 * blk, x_half), F32)]
+    scratch += [vm((x_half // 128, 24, 128), F32)] * 2
+    scratch += [vm((2 * hp, 2 * blk, STATE), F32), vm((x_total // 128, blk, 128), F32)]
+    scratch += [vm((x_half // 128, 2 * blk, 128), BF16), vm((2 * hp, STATE, 2 * blk), BF16)]
+    scratch += [vm((2 * hp, 2 * blk, 128), BF16), vm((x_half // 128, 2 * blk, 128), F32)]
     scratch += [vm((tiles, 4, 2, STATE, 128), BF16)] * 4
     scratch += [vm((8, 128), F32), vm((4, 8, 128), F32), vm((8, 128), F32), vm((nz, 8, 128), F32)]
     scratch += [vm((4, 2, tiles, 8, 128), F32)] * 2 + [vm((2, tiles, 8, 128), F32)]
@@ -1222,7 +1259,7 @@
     dma = pltpu.SemaphoreType.DMA
     scratch += [dma((16,)), dma((2, 5, 2)), dma((2, 3, 2)), dma((2, 3)), dma((2, 3))]
     scratch += [dma((2, 4)), dma((2, nz)), dma((2, tiles, 4)), dma((rounds, tiles, nz))]
-    scratch += [dma((rounds, tiles)), dma((2, tiles, 4)), dma((2, tiles, hp))]
+    scratch += [dma((rounds, tiles)), dma((2, tiles, 4)), dma((2, tiles))]
     out = pl.pallas_call(
         functools.partial(quad_kernel, (heads, pairs, sp, dp)),
         out_shape=pltpu.VMEM((blk, x_total), BF16),

time: 40.1 us -> 39.2 us (0.978)
  Pallas kernels: 39 us -> 38.1 us
    pallas_call x1, Pallas kernels: 39 us -> 38.1 us  [quad_local(): pl.pallas_call(functools.partial(quad_kernel, (heads, pairs, sp, dp)), ou...]
where the time goes in v3:
time: 39.2 us; the launch traced here: 39 us
  Pallas kernels  38.1 us (97%)
  local copies, waits for them, and re-layouts  0.88 us (2%)
    pallas_call x1, Pallas kernels, quad_local(): pl.pallas_call(functools.partial(quad_kernel, (heads, pairs, sp, dp)), ou...  38.1 us
    unnamed x1, local copies, waits for them, and re-layouts  0.88 us

profile of v3, /device:TPU:0, one launch (start us, length us, event | category | flops | bytes accessed | tf_op | source)
XLA Modules:
  0.0 39.0 jit_solution(3489481489205385114)
XLA Ops:
  0.0 38.1 %mixer.1 = bf16[128,3072]{1,0:T(8,128)(2,1)S(1)} custom-call(bf16[128,3072]{1,0:T(8,128)(2,1)} %bitcast.16, bf16[128,2048]{1,0:T(8,128)(2,1)} %bitcast.18, bf16[128,2048]{1,0:T(8,128)(2,1)} %bitcast.19, bf16[128,3072]{1,0:T(8,128)(2,1)} %bitcast.17, f32[48,128]{1,0:T(8,128)} %bitcast.20, f32[48,128]{1,0:T(8,128)} %bitcast.21, f32[48,128]{1,0:T(8,128)} %bitcast.22, ...), custom_call_target="tpu_custom_call" | custom-call | tf_op jit(solution)/shard_map/mixer/pallas_call | solution.py:1263
  38.1 0.9 %copy.15 = bf16[1,128,3072]{2,1,0:T(8,128)(2,1)} copy(bf16[1,128,3072]{2,1,0:T(8,128)(2,1)S(1)} %bitcast.15) | data formatting | bytes 1572864

commit v4 on v3

--- a/solution.py
+++ b/solution.py
@@ -568,10 +568,11 @@
     gain_hbm, out_ref = refs[12:14]
     (in_x, in_b, in_c, in_z, inc, inc_out, gain_in, px, pb, pc) = refs[14:24]
     own, got = refs[24:29], refs[29:34]
-    edges = refs[34:40]
+    edge_out, low_in, high_in = refs[34:37]
+    refs = refs[:37] + (None,) * 3 + refs[37:]
     (work, w_ref, prm_ref, gain_ref, cum_ref, fac_ref, col_ref, cum_t, rate_t, mid_t) = refs[40:50]
-    low_ref, high_ref, bc, zg = refs[50:54]
-    refs = refs[:50] + refs[54:]
+    low_ref, high_ref, bc, zg, wide_cum = refs[50:55]
+    refs = refs[:50] + refs[55:]
     (xc, bt, cc, y_ref, sup, up_in, down_out, down_in) = refs[50:58]
     (logs, qlog, zsum, zlog, dec, wup, zdec, zwt) = refs[58:66]
     (tz, zin, zs, zr, mix_out, mix_in) = refs[66:72]
@@ -697,15 +698,12 @@
     sources = (in_x, in_b, in_c)
     halves = (x_half, b_half, b_half)
 
-    def edge_copy(i, low, k):
-        half = halves[i]
-        start = blk - EDGE if low else 0
+    edge_from = (0, x_half // 128, (x_half + b_half) // 128)
+
+    def edge_copy(low, k):
         return remote(
-            sources[i].at[pl.ds(start, EDGE), pl.ds(k * half, half)],
-            edges[i if low else 3 + i],
-            edge_sem.at[0, i, k],
-            edge_sem.at[1, i, 0 if low else 1],
-            chip_id(after if low else before, k),
+            edge_out.at[k], low_in if low else high_in, edge_sem.at[0, k],
+            edge_sem.at[1, 0 if low else 1], chip_id(after if low else before, k),
         )
 
     sends_low = jnp.logical_and(core == 1, has_next)
@@ -717,19 +715,30 @@
             sources[i].at[:, cut], (px, pb, pc)[i], half_sem.at[0, i], half_sem.at[1, i], partner
         )
 
-    for i, one in ((1, b_load), (0, x_load), (2, c_load)):
+    for one in (b_load, x_load, c_load):
         one.wait()
-
-        @pl.when(sends_low)
-        def _(i=i):
+    slab = edge_out.shape[2]
+    for k in range(2):
+        picked = [[], []]
+        for i in range(3):
+            for t in range(halves[i] // 128):
+                at = slice(k * halves[i] + t * 128, k * halves[i] + (t + 1) * 128)
+                end = sources[i][blk - EDGE :, at].astype(F32)[EDGE - 2 :]
+                start = sources[i][0:EDGE, at].astype(F32)[0:2]
+                both = jnp.where(core == 1, end, start)
+                for r in range(2):
+                    picked[r].append(both[r : r + 1])
+        for r in range(2):
+            spare = jnp.zeros((slab - len(picked[r]), 128), F32)
+            edge_out[k, r] = jnp.concatenate(picked[r] + [spare], axis=0).astype(BF16)
+    for low, sends in ((True, sends_low), (False, sends_high)):
+
+        @pl.when(sends)
+        def _(low=low):
             for k in range(2):
-                edge_copy(i, True, k).start()
-
-        @pl.when(sends_high)
-        def _(i=i):
-            for k in range(2):
-                edge_copy(i, False, k).start()
-
+                edge_copy(low, k).start()
+
+    for i in (1, 0):
         half_copy(i).start()
 
     lane = lax.broadcasted_iota(jnp.int32, (blk, 128), 1)
@@ -813,9 +822,12 @@
     gain_load.wait()
     gain_ref[...] = gain_in[...].astype(F32)
 
-    for i in range(3):
-        remote(sources[i].at[:, pl.ds(0, halves[i])], (px, pb, pc)[i], half_sem.at[0, i],
-               half_sem.at[1, i], partner).wait_recv()
+    def half_wait(i):
+        remote(
+            sources[i].at[:, pl.ds(0, halves[i])], (px, pb, pc)[i], half_sem.at[0, i],
+            half_sem.at[1, i], partner,
+        ).wait_recv()
+
     def rolled(v, p):
         return pltpu.roll(v, lax.rem(128 - p * per_pair, 128), 1)
 
@@ -836,9 +848,10 @@
         else:
             (xc, None, cc)[i][t, rows, :] = v.astype(BF16)
 
-    def conv(i, group, _):
-        for spot in range(4):
-            t = group * 4 + spot
+    def conv(i, k, base):
+        for p in range(hp):
+            t = p * (tiles_of[i] // hp) + k
+            spot = base + p
             mine_at = pl.ds(pl.multiple_of(core * halves[i] + t * 128, 128), 128)
             at = pl.ds(pl.multiple_of(t * 128, 128), 128)
             buf = work.at[spot]
@@ -847,34 +860,40 @@
             buf[here_at, :] = sources[i][:, mine_at].astype(F32)
             buf[there_at, :] = (px, pb, pc)[i][:, at].astype(F32)
             s = buf[6 : 6 + tokens, :] * w_ref[starts[i] + t, 0:1, :]
-            for k in range(1, 4):
-                s = s + buf[6 + k : 6 + k + tokens, :] * w_ref[starts[i] + t, k : k + 1, :]
+            for tap in range(1, 4):
+                near = buf[6 + tap : 6 + tap + tokens, :]
+                s = s + near * w_ref[starts[i] + t, tap : tap + 1, :]
             store(i, t, slice(0, tokens), silu(s))
-        return 0
-
-    def edge_wait(i):
+
+    def edge_wait():
         for low, present in ((True, has_prev), (False, has_next)):
 
             @pl.when(present)
             def _(low=low):
-                edge_copy(i, low, 0).wait_recv()
-
-    def fix(i):
+                edge_copy(low, 0).wait_recv()
+
+    def fix(i, k):
         half = halves[i]
+        mine_tiles = [p * (tiles_of[i] // hp) + k for p in range(hp)]
         row16 = row[0:16]
+        lows = [low_in[r].astype(F32) for r in range(2)]
+        highs = high_in[0].astype(F32)
         own_part = sources[i]
         their_part = (px, pb, pc)[i]
-        for t in range(tiles_of[i]):
+        for t in mine_tiles:
             mine_at = pl.ds(pl.multiple_of(core * half + t * 128, 128), 128)
             at = slice(t * 128, (t + 1) * 128)
             start = jnp.where(core == 0, own_part[0:8, mine_at], their_part[0:8, at])
             end = jnp.where(core == 1, own_part[blk - 8 :, mine_at], their_part[blk - 8 :, at])
-            low_ref[t, 0:8, :] = jnp.where(has_prev, edges[i][:, at].astype(F32), 0.0)
+            e = edge_from[i] + t
+            for r in range(2):
+                before_row = jnp.where(has_prev, lows[r][e : e + 1], 0.0)
+                low_ref[t, 6 + r : 7 + r, :] = before_row
             low_ref[t, 8:16, :] = start.astype(F32)
             high_ref[t, 8:16, :] = end.astype(F32)
-            high_ref[t, 16:24, :] = jnp.where(has_next, edges[3 + i][:, at].astype(F32), 0.0)
+            high_ref[t, 16:17, :] = jnp.where(has_next, highs[e : e + 1], 0.0)
         dst = (xc, bc, cc)[i]
-        for t in range(tiles_of[i]):
+        for t in mine_tiles:
             for ref, low in ((low_ref, True), (high_ref, False)):
                 s = ref[t, 6:14, :] * w_ref[starts[i] + t, 0:1, :]
                 for k in range(1, 4):
@@ -885,25 +904,23 @@
                 keep = row16 >= 2 if low else row16 < 15
                 store(i, t, rows, jnp.where(keep, dst[t, rows, :].astype(F32), s))
 
-    def up_copy(k, i):
+    def up_copy(k, d, i):
         qy, qx, q = member(i)
         return remote(
-            sup.at[k, q], up_in.at[k, me], up_sem.at[0, k, i], up_sem.at[1, k, me],
-            quad_id(qy, qx),
+            sup.at[k, q, d], up_in.at[k, me, d], up_sem.at[0, 2 * k + d, i],
+            up_sem.at[1, 2 * k + d, me], quad_id(qy, qx),
         )
 
     def wide_left(n):
         return lax.rem(lax.broadcasted_iota(jnp.int32, (128, n), 1), 128) < HEAD_DIM
 
     def first(k):
-        fac = fac_ref[...]
         for p in range(hp):
             if k < 2:
                 bt[2 * p + k] = bc[2 * p + k].T.astype(BF16)
             xf = xc[p * tiles + k].astype(F32)
-            head = p * per_pair + 2 * k
             rhs = jnp.concatenate(
-                [(xf * two(fac, d * hh + head)).astype(BF16) for d in range(2)], axis=1
+                [(xf * wide_cum[k, p, d]).astype(BF16) for d in range(2)], axis=1
             )
             u = jnp.dot(bt[2 * p + k // 2], rhs, preferred_element_type=F32)
             if k == 1:
@@ -912,46 +929,45 @@
             u = u.astype(BF16)
             sup[k, p, 0] = u[:, :128]
             sup[k, p, 1] = u[:, 128:]
-        for i in range(3):
-            up_copy(k, i).start()
+        for d in range(2):
+            for i in range(3):
+                up_copy(k, d, i).start()
         up_in[k, me] = sup[k, me]
 
-    def inner(p, _):
-        for r in range(2):
-            rows = slice(r * blk, (r + 1) * blk)
-            cols = rolled(col_ref[rows, :], p)
-            mid_row = mid_f if r == 1 else mid_b
-            shift = rolled(jnp.exp(jnp.minimum(col_ref[rows, :] - mid_row, 0.0)), p)
-            parts = []
-            for g in range(2):
-                scores = jnp.dot(cc[2 * p + g, rows], bt[2 * p + g], preferred_element_type=F32)
-                on = scores[:, r * blk : (r + 1) * blk]
-                away = scores[:, (1 - r) * blk : (2 - r) * blk]
-                for h in range(g * per_pair // 2, (g + 1) * per_pair // 2):
-                    f = pl.ds(p * per_pair + h, 1)
-                    b = pl.ds(hh + p * per_pair + h, 1)
-                    gap_f = cols[:, h : h + 1] - cum_t[f, rows]
-                    gap_b = cols[:, hh + h : hh + h + 1] - cum_t[b, rows]
-                    gap = jnp.where(lane < row, gap_f, jnp.where(lane > row, gap_b, 0.0))
-                    rf, rb = rate_t[f, rows], rate_t[b, rows]
-                    scale = jnp.where(lane < row, rf, jnp.where(lane > row, rb, rf + rb))
-                    near = (on * jnp.exp(gap) * scale).astype(BF16)
-                    d = 1 - r
-                    c = d * hh + h
-                    far_rows = slice((1 - r) * blk, (2 - r) * blk)
-                    far_row = mid_t[f if d == 0 else b, far_rows]
-                    far = (away * shift[:, c : c + 1] * far_row).astype(BF16)
-                    parts.append(jnp.concatenate([near, far] if r == 0 else [far, near], axis=1))
-            for k in range(tiles):
-                xt = xc[p * tiles + k]
-                zero = jnp.zeros_like(xt)
-                mask = lax.broadcasted_iota(jnp.int32, xt.shape, 1) < HEAD_DIM
-                both = jnp.concatenate(
-                    [jnp.where(mask, xt, zero), jnp.where(mask, zero, xt)], axis=0
-                )
-                w = jnp.concatenate([parts[2 * k], parts[2 * k + 1]], axis=1)
-                y_ref[p * tiles + k, rows] = jnp.dot(w, both, preferred_element_type=F32)
-        return 0
+    def inner(p, r):
+        rows = slice(r * blk, (r + 1) * blk)
+        cols = rolled(col_ref[rows, :], p)
+        mid_row = mid_f if r == 1 else mid_b
+        shift = rolled(jnp.exp(jnp.minimum(col_ref[rows, :] - mid_row, 0.0)), p)
+        parts = []
+        for g in range(2):
+            scores = jnp.dot(cc[2 * p + g, rows], bt[2 * p + g], preferred_element_type=F32)
+            on = scores[:, r * blk : (r + 1) * blk]
+            away = scores[:, (1 - r) * blk : (2 - r) * blk]
+            for h in range(g * per_pair // 2, (g + 1) * per_pair // 2):
+                f = pl.ds(p * per_pair + h, 1)
+                b = pl.ds(hh + p * per_pair + h, 1)
+                gap_f = cols[:, h : h + 1] - cum_t[f, rows]
+                gap_b = cols[:, hh + h : hh + h + 1] - cum_t[b, rows]
+                gap = jnp.where(lane < row, gap_f, jnp.where(lane > row, gap_b, 0.0))
+                rf, rb = rate_t[f, rows], rate_t[b, rows]
+                scale = jnp.where(lane < row, rf, jnp.where(lane > row, rb, rf + rb))
+                near = (on * jnp.exp(gap) * scale).astype(BF16)
+                d = 1 - r
+                c = d * hh + h
+                far_rows = slice((1 - r) * blk, (2 - r) * blk)
+                far_row = mid_t[f if d == 0 else b, far_rows]
+                far = (away * shift[:, c : c + 1] * far_row).astype(BF16)
+                parts.append(jnp.concatenate([near, far] if r == 0 else [far, near], axis=1))
+        for k in range(tiles):
+            xt = xc[p * tiles + k]
+            zero = jnp.zeros_like(xt)
+            mask = lax.broadcasted_iota(jnp.int32, xt.shape, 1) < HEAD_DIM
+            both = jnp.concatenate(
+                [jnp.where(mask, xt, zero), jnp.where(mask, zero, xt)], axis=0
+            )
+            w = jnp.concatenate([parts[2 * k], parts[2 * k + 1]], axis=1)
+            y_ref[p * tiles + k, rows] = jnp.dot(w, both, preferred_element_type=F32)
 
     def zlog_copy(o):
         return remote(
@@ -973,6 +989,7 @@
         zlog[cz] = zsum[...]
         for d in range(2):
             for k in range(tiles):
+                zdec[d, k] = jnp.exp(lanes_of(zsum[...], d, k))
                 each = [lanes_of(qlog[q], d, k) for q in range(4)]
                 reach = jnp.zeros_like(each[0])
                 for q in reversed(range(4)) if d == 0 else range(4):
@@ -998,22 +1015,22 @@
                 reach[r][1] = reach[r][1] + jnp.where(b_in, zlog[s], 0.0)
         for d in range(2):
             for k in range(tiles):
-                zdec[d, k] = jnp.exp(lanes_of(zsum[...], d, k))
                 for r in range(rounds):
                     zwt[r, d, k] = jnp.exp(lanes_of(reach[r][d], d, k))
 
-    def combine(k):
+    def combine(k, d):
         for i in range(3):
             _, _, q = member(i)
             remote(
-                sup.at[k, q], up_in.at[k, q], up_sem.at[0, k, i], up_sem.at[1, k, q], partner
+                sup.at[k, q, d], up_in.at[k, q, d], up_sem.at[0, 2 * k + d, i],
+                up_sem.at[1, 2 * k + d, q], partner,
             ).wait_recv()
-        for d in range(2):
-            acc = up_in[k, 0, d].astype(F32) * wup[0, d, k, 0:1, :]
-            for q in range(1, 4):
-                acc = acc + up_in[k, q, d].astype(F32) * wup[q, d, k, 0:1, :]
-            tz[k, d] = acc
-            zin[k, d] = jnp.zeros_like(acc)
+        acc = up_in[k, 0, d].astype(F32) * wup[0, d, k, 0:1, :]
+        for q in range(1, 4):
+            acc = acc + up_in[k, q, d].astype(F32) * wup[q, d, k, 0:1, :]
+        tz[k, d] = acc
+        zin[k, d] = jnp.zeros_like(acc)
+        z_send(0, k, d)
 
     def z_copy(r, k, o, d):
         return remote(
@@ -1026,43 +1043,47 @@
         pos = lax.rem(cz, 2 * h)
         return h, pos, ((0, pos == h - 1), (1, pos == h))
 
-    def z_send(r, k):
-        h, pos, senders = z_parts(r)
-        for d, sender in senders:
-
-            @pl.when(sender)
-            def _(d=d):
-                zs[r, k] = (zin[k, d] * zdec[d, k, 0:1, :] + tz[k, d]).astype(BF16)
-                for o in reversed(range(1, h + 1)):
-                    z_copy(r, k, o, d).start()
-
-    def z_recv(r, k):
+    def z_send(r, k, d):
+        h, _, senders = z_parts(r)
+
+        @pl.when(senders[d][1])
+        def _():
+            zs[r, k] = (zin[k, d] * zdec[d, k, 0:1, :] + tz[k, d]).astype(BF16)
+            for o in reversed(range(1, h + 1)):
+                z_copy(r, k, o, d).start()
+
+    def z_recv(r, k, d):
         h, pos, _ = z_parts(r)
-        z_copy(r, k, 1, 0).wait_recv()
-        for d, receiver in ((0, pos >= h), (1, pos < h)):
-
-            @pl.when(receiver)
-            def _(d=d):
-                zin[k, d] = zin[k, d] + zr[r, k].astype(F32) * zwt[r, d, k, 0:1, :]
-
-    def down_copy(k, i):
+
+        @pl.when(pos >= h if d == 0 else pos < h)
+        def _():
+            remote(
+                zs.at[r, k], zr.at[r, k], zsend_sem.at[r, k, 0], zrecv_sem.at[r, k], partner
+            ).wait_recv()
+            zin[k, d] = zin[k, d] + zr[r, k].astype(F32) * zwt[r, d, k, 0:1, :]
+
+        if r + 1 < rounds:
+            z_send(r + 1, k, d)
+        else:
+            down(k, d)
+
+    def down_copy(k, d, i):
         qy, qx, q = member(i)
         return remote(
-            down_out.at[k, q], down_in.at[k, me], down_sem.at[0, k, i], down_sem.at[1, k, me],
-            quad_id(qy, qx),
-        )
-
-    def down(k):
-        for d in range(2):
-            g = zin[k, d]
-            order = list(range(4)) if d == 0 else list(reversed(range(4)))
-            for q in order:
-                down_out[k, q, d] = g.astype(BF16)
-                if q != order[-1]:
-                    g = g * dec[q, d, k, 0:1, :] + up_in[k, q, d].astype(F32)
+            down_out.at[k, q, d], down_in.at[k, me, d], down_sem.at[0, 2 * k + d, i],
+            down_sem.at[1, 2 * k + d, me], quad_id(qy, qx),
+        )
+
+    def down(k, d):
+        g = zin[k, d]
+        order = list(range(4)) if d == 0 else list(reversed(range(4)))
+        for q in order:
+            down_out[k, q, d] = g.astype(BF16)
+            if q != order[-1]:
+                g = g * dec[q, d, k, 0:1, :] + up_in[k, q, d].astype(F32)
         for i in range(3):
-            down_copy(k, i).start()
-        down_in[k, me] = down_out[k, me]
+            down_copy(k, d, i).start()
+        down_in[k, me, d] = down_out[k, me, d]
 
     def gates(group, _):
         for spot in range(4):
@@ -1085,25 +1106,33 @@
             mix_out.at[k], mix_in.at[k], mix_sem.at[0, k], mix_sem.at[1, k], partner
         )
 
+    def spread(k, ref=cum_ref):
+        for j in range(2):
+            cols = ref[j * blk : (j + 1) * blk, :]
+            for p in range(hp):
+                head = p * per_pair + 2 * k
+                for d in range(2):
+                    wide_cum[k, p, d, j * blk : (j + 1) * blk, :] = two(cols, d * hh + head)
+
     def last(k):
         for i in range(3):
             _, _, q = member(i)
-            remote(
-                down_out.at[k, q], down_in.at[k, q], down_sem.at[0, k, i], down_sem.at[1, k, q],
-                partner,
-            ).wait_recv()
+            for d in range(2):
+                remote(
+                    down_out.at[k, q, d], down_in.at[k, q, d], down_sem.at[0, 2 * k + d, i],
+                    down_sem.at[1, 2 * k + d, q], partner,
+                ).wait_recv()
         for mine in (False, True):
             rows = pl.ds(pl.multiple_of((core if mine else other) * blk, 128), blk)
-            cols = cum_ref[rows, :]
             for p in range(hp):
                 rhs = jnp.concatenate([down_in[k, p, 0], down_in[k, p, 1]], axis=1)
                 v = jnp.dot(cc[2 * p + k // 2, rows], rhs, preferred_element_type=F32)
                 if k == 1:
                     u = jnp.dot(cc[2 * p + 1, rows], rhs, preferred_element_type=F32)
                     v = jnp.where(wide_left(256), v, u)
-                head = p * per_pair + 2 * k
                 t = p * tiles + k
-                y = y_ref[t, rows] + v[:, :128] * two(cols, head) + v[:, 128:] * two(cols, hh + head)
+                y = y_ref[t, rows] + v[:, :128] * wide_cum[k, p, 0, rows]
+                y = y + v[:, 128:] * wide_cum[k, p, 1, rows]
                 mixed = y.astype(BF16)
                 if mine:
                     gate(mixed, core * tiles_of[0] + t)
@@ -1117,65 +1146,64 @@
         for p in range(hp):
             gate(mix_in[k, p], other * tiles_of[0] + p * tiles + k)
 
-    for spot in range(4):
+    for spot in range(2 * hp):
         work[spot, 0:8, :] = jnp.zeros((8, 128), F32)
         work[spot, 8 + tokens :, :] = jnp.zeros((8, 128), F32)
     low_ref[...] = jnp.zeros_like(low_ref)
     high_ref[...] = jnp.zeros_like(high_ref)
-    for i in (1, 0):
-        lax.fori_loop(0, tiles_of[i] // 4, functools.partial(conv, i), 0)
+    half_copy(2).start()
+    spread(0, fac_ref)
+    half_wait(1)
+    conv(1, 0, 0)
+    half_wait(0)
+    conv(0, 0, hp)
+    edge_wait()
+    fix(1, 0)
+    fix(0, 0)
+    first(0)
+    spread(1, fac_ref)
+    conv(1, 1, 0)
+    conv(0, 1, hp)
+    fix(1, 1)
+    fix(0, 1)
+    first(1)
+    spread(2, fac_ref)
+    conv(0, 2, 0)
+    fix(0, 2)
+    first(2)
     quad_logs()
-    for i in (1, 0):
-        edge_wait(i)
-    for i in (1, 0):
-        fix(i)
-    first(0)
-    first(1)
-    first(2)
-    lax.fori_loop(0, tiles_of[2] // 4, functools.partial(conv, 2), 0)
-    edge_wait(2)
-    fix(2)
-    z_logs()
-    combine(0)
-    z_send(0, 0)
-    lax.fori_loop(0, 1, inner, 0)
-    z_recv(0, 0)
-    for r in range(1, rounds):
-        z_send(r, 0)
-        if r < rounds - 1:
-            z_recv(r, 0)
-    combine(1)
-    z_send(0, 1)
-    lax.fori_loop(1, 2, inner, 0)
-    z_recv(0, 1)
-    for r in range(1, rounds):
-        z_send(r, 1)
-        if r < rounds - 1:
-            z_recv(r, 1)
-    combine(2)
-    z_send(0, 2)
-    if rounds > 1:
-        z_recv(rounds - 1, 0)
-    down(0)
-    lax.fori_loop(2, 3, inner, 0)
-    z_recv(0, 2)
-    for r in range(1, rounds):
-        z_send(r, 2)
-        if r < rounds - 1:
-            z_recv(r, 2)
-    if rounds > 1:
-        z_recv(rounds - 1, 1)
-    down(1)
-    lax.fori_loop(3, hp, inner, 0)
-    if rounds > 1:
-        z_recv(rounds - 1, 2)
-    down(2)
+    half_wait(2)
+    for k in range(2):
+        conv(2, k, k * hp)
+    for k in range(2):
+        fix(2, k)
     z_load.wait()
-    lax.fori_loop(0, 2 * tiles_of[0] // 4, gates, 0)
+
+    up_step, z_first, z_next = 1.4, 2.7, 3.5
+    plan = [(z_first - 0.01, z_logs)]
     for k in range(3):
-        last(k)
-        if k > 0:
-            finish(k - 1)
+        for d in range(2):
+            when = up_step * (2 * k + d)
+            plan.append((when, functools.partial(combine, k, d)))
+            for r in range(rounds):
+                plan.append((when + z_first + r * z_next, functools.partial(z_recv, r, k, d)))
+    for p in range(hp):
+        for r in range(2):
+            plan.append((up_step * p + 0.1 + 0.01 * r, functools.partial(inner, p, r)))
+    all_gates = functools.partial(
+        lax.fori_loop, 0, 2 * tiles_of[0] // 4, gates, 0
+    )
+    plan.append((up_step * hp + 0.1, all_gates))
+    done = z_first + (rounds - 1) * z_next
+    for k in range(3):
+        plan.append((done + up_step * k + 0.1, functools.partial(spread, k)))
+    for _, step in sorted(plan, key=lambda one: one[0]):
+        step()
+    last(0)
+    last(1)
+    finish(0)
+    last(2)
+    finish(1)
     finish(2)
 
     for x in range(2):
@@ -1189,9 +1217,8 @@
 
         @pl.when(sends)
         def _(low=low):
-            for i in range(3):
-                for k in range(2):
-                    edge_copy(i, low, k).wait_send()
+            for k in range(2):
+                edge_copy(low, k).wait_send()
 
     for i in range(3):
         inc_copy(i).wait_send()
@@ -1201,8 +1228,9 @@
         zlog_copy(o).wait_send()
     for k in range(3):
         for i in range(3):
-            up_copy(k, i).wait_send()
-            down_copy(k, i).wait_send()
+            for d in range(2):
+                up_copy(k, d, i).wait_send()
+                down_copy(k, d, i).wait_send()
         mix_copy(k).wait_send()
         for r in range(rounds):
             h, _, senders = z_parts(r)
@@ -1234,6 +1262,7 @@
     hp, hh = pairs // 2, heads // 2
     x_half, b_half = x_total // 2, b_total // 2
     width = x_half + 2 * b_half
+    slab = pl.cdiv(width // 128, 16) * 16
     params = (wx, wb, wc, offset, fading)
     vm = pltpu.VMEM
     gains = gain.reshape(x_total // 128, 128)
@@ -1242,12 +1271,13 @@
     scratch += [vm((blk, x_half), BF16), vm((blk, b_half), BF16), vm((blk, b_half), BF16)]
     scratch += [vm(one.shape, one.dtype) for one in params]
     scratch += [vm((2,) + one.shape, one.dtype) for one in params]
-    scratch += [vm((EDGE, n), BF16) for n in (x_half, b_half, b_half)] * 2
-    scratch += [vm((4, 2 * blk + 16, 128), F32), vm((width // 128, 8, 128), F32)]
+    scratch += [vm((2, 2, slab, 128), BF16)] + [vm((2, slab, 128), BF16)] * 2
+    scratch += [vm((2 * hp, 2 * blk + 16, 128), F32), vm((width // 128, 8, 128), F32)]
     scratch += [vm((8, 128), F32), vm(gains.shape, F32)] + [vm((2 * blk, 128), F32)] * 3
     scratch += [vm((128, 2 * blk), F32)] * 3
     scratch += [vm((x_half // 128, 24, 128), F32)] * 2
     scratch += [vm((2 * hp, 2 * blk, STATE), F32), vm((x_total // 128, blk, 128), F32)]
+    scratch += [vm((tiles, hp, 2, 2 * blk, 128), F32)]
     scratch += [vm((x_half // 128, 2 * blk, 128), BF16), vm((2 * hp, STATE, 2 * blk), BF16)]
     scratch += [vm((2 * hp, 2 * blk, 128), BF16), vm((x_half // 128, 2 * blk, 128), F32)]
     scratch += [vm((tiles, 4, 2, STATE, 128), BF16)] * 4
@@ -1257,9 +1287,9 @@
     scratch += [vm((tiles, 2, STATE, 128), F32)] * 2 + [vm((rounds, tiles, STATE, 128), BF16)] * 2
     scratch += [vm((tiles, hp, blk, 128), BF16)] * 2
     dma = pltpu.SemaphoreType.DMA
-    scratch += [dma((16,)), dma((2, 5, 2)), dma((2, 3, 2)), dma((2, 3)), dma((2, 3))]
-    scratch += [dma((2, 4)), dma((2, nz)), dma((2, tiles, 4)), dma((rounds, tiles, nz))]
-    scratch += [dma((rounds, tiles)), dma((2, tiles, 4)), dma((2, tiles))]
+    scratch += [dma((16,)), dma((2, 5, 2)), dma((2, 2)), dma((2, 3)), dma((2, 3))]
+    scratch += [dma((2, 4)), dma((2, nz)), dma((2, 2 * tiles, 4)), dma((rounds, tiles, nz))]
+    scratch += [dma((rounds, tiles)), dma((2, 2 * tiles, 4)), dma((2, tiles))]
     out = pl.pallas_call(
         functools.partial(quad_kernel, (heads, pairs, sp, dp)),
         out_shape=pltpu.VMEM((blk, x_total), BF16),

time: 39.2 us -> 36.1 us (0.921)
  Pallas kernels: 38.1 us -> 34.8 us
    pallas_call x1, Pallas kernels: 38.1 us -> 34.8 us  [quad_local(): pl.pallas_call(functools.partial(quad_kernel, (heads, pairs, sp, dp)), ou...]
where the time goes in v4:
time: 36.1 us; the launch traced here: 35.7 us
  Pallas kernels  34.8 us (96%)
  local copies, waits for them, and re-layouts  0.88 us (2%)
    pallas_call x1, Pallas kernels, quad_local(): pl.pallas_call(functools.partial(quad_kernel, (heads, pairs, sp, dp)), ou...  34.8 us
    unnamed x1, local copies, waits for them, and re-layouts  0.88 us

profile of v4, /device:TPU:0, one launch (start us, length us, event | category | flops | bytes accessed | tf_op | source)
XLA Modules:
  0.0 35.7 jit_solution(7054759499285850026)
XLA Ops:
  0.0 34.8 %mixer.1 = bf16[128,3072]{1,0:T(8,128)(2,1)S(1)} custom-call(bf16[128,3072]{1,0:T(8,128)(2,1)} %bitcast.16, bf16[128,2048]{1,0:T(8,128)(2,1)} %bitcast.18, bf16[128,2048]{1,0:T(8,128)(2,1)} %bitcast.19, bf16[128,3072]{1,0:T(8,128)(2,1)} %bitcast.17, f32[48,128]{1,0:T(8,128)} %bitcast.20, f32[48,128]{1,0:T(8,128)} %bitcast.21, f32[48,128]{1,0:T(8,128)} %bitcast.22, ...), custom_call_target="tpu_custom_call" | custom-call | tf_op jit(solution)/shard_map/mixer/pallas_call | solution.py:1293
  34.9 0.9 %copy.15 = bf16[1,128,3072]{2,1,0:T(8,128)(2,1)} copy(bf16[1,128,3072]{2,1,0:T(8,128)(2,1)S(1)} %bitcast.15) | data formatting | bytes 1572864

commit v5 on v4

--- a/solution.py
+++ b/solution.py
@@ -652,16 +652,23 @@
     mine = pl.ds(pl.multiple_of(core * hh, 8), hh)
     theirs = pl.ds(pl.multiple_of(other * hh, 8), hh)
     raw = (ahead_hbm, back_hbm, spike_hbm)
-    inc_stage = [load(raw[i].at[theirs, :], inc_out.at[i]) for i in range(3)]
-    inc_loads = [load(raw[i].at[mine, :], inc.at[core, i]) for i in range(3)]
+    for i in range(3):
+        pltpu.make_async_copy(raw[i].at[theirs, :], inc_out.at[i], load_sem.at[10]).start()
+        pltpu.make_async_copy(raw[i].at[mine, :], inc.at[core, i], load_sem.at[11]).start()
     b_load = load(b_hbm, in_b)
     x_load = load(x_hbm, in_x)
     c_load = load(c_hbm, in_c)
     gain_load = load(gain_hbm, gain_in)
     z_load = load(z_hbm, in_z)
 
-    for one in param_loads + inc_stage:
+    for spot in range(2 * hp):
+        work[spot, 0:8, :] = jnp.zeros((8, 128), F32)
+        work[spot, 8 + tokens :, :] = jnp.zeros((8, 128), F32)
+    low_ref[...] = jnp.zeros_like(low_ref)
+    high_ref[...] = jnp.zeros_like(high_ref)
+    for one in param_loads:
         one.wait()
+    pltpu.make_async_copy(inc_out, inc_out, load_sem.at[10]).wait()
     chip_greets = 2 * ((chip + chips - 1) // chips + (2 * chips - 2 - chip) // chips)
     pl.semaphore_wait(barrier, (sp - 1) + 3 + (nz - 1) + chip_greets)
 
@@ -687,13 +694,8 @@
             for i in range(5):
                 got[i][slot] = own[i][...]
 
-    def inc_copy(i):
-        return remote(
-            inc_out.at[i], inc.at[core, i], inc_sem.at[0, i], inc_sem.at[1, i], partner
-        )
-
-    for i in range(3):
-        inc_copy(i).start()
+    inc_copy = remote(inc_out, inc.at[core], inc_sem.at[0], inc_sem.at[1], partner)
+    inc_copy.start()
 
     sources = (in_x, in_b, in_c)
     halves = (x_half, b_half, b_half)
@@ -759,68 +761,8 @@
                     own[i], got[i].at[q], prm_sem.at[0, i, 0], prm_sem.at[1, i, q], partner
                 ).wait_recv()
 
-    for one in inc_loads:
-        one.wait()
-    for i in range(3):
-        remote(
-            inc_out.at[i], inc.at[other, i], inc_sem.at[0, i], inc_sem.at[1, i], partner
-        ).wait_recv()
-    prm_ref[...] = jnp.zeros_like(prm_ref)
-    wide = own[3].shape[1]
-    for q in range(2):
-        for kind in range(2):
-            for d in range(2):
-                at = slice(d * hh + q * wide, d * hh + (q + 1) * wide)
-                prm_ref[kind : kind + 1, at] = got[3 + kind][q, d : d + 1, :]
-        off = 0
-        for i in range(3):
-            n = own[i].shape[1]
-            part = got[i][q].astype(F32)
-            for t in range(n // 128):
-                w_ref[off + q * (n // 128) + t, 0:4, :] = part[:, t * 128 : (t + 1) * 128]
-            off += 2 * n // 128
-
-    cums, rates = [], []
-    for j in range(2):
-        pre = jnp.concatenate([inc[j, 0], inc[j, 1], filler], axis=0).T
-        spikes = jnp.concatenate([inc[j, 2], inc[j, 2], filler], axis=0).T
-        rate = jax.nn.softplus(pre + prm_ref[0:1, :])
-        log_decay = -jnp.exp(prm_ref[1:2, :]) * rate + spikes
-        cum_f = jnp.dot(lower, log_decay, precision=HIGHEST, preferred_element_type=F32)
-        cum_b = jnp.dot(upper, log_decay, precision=HIGHEST, preferred_element_type=F32)
-        cums.append((cum_f, cum_b))
-        rates.append(rate)
-    ahead_lane = lane < hh
-    ahead1 = ahead_lane[0:1]
-    mid_f, mid_b = cums[0][0][blk - 1 : blk], cums[1][1][0:1]
-    total = jnp.where(ahead1, mid_f + cums[1][0][blk - 1 : blk], cums[0][1][0:1] + mid_b)
-    logs[...] = jnp.broadcast_to(total, (8, 128))
-
-    def qlog_copy(i):
-        qy, qx, q = member(i)
-        return remote(
-            logs, qlog.at[me], qlog_sem.at[0, i], qlog_sem.at[1, me], quad_id(qy, qx)
-        )
-
-    for i in range(3):
-        qlog_copy(i).start()
-    qlog[me] = logs[...]
-    for j in range(2):
-        cum_f, cum_b = cums[j]
-        far = jnp.where(ahead_lane, mid_f if j == 1 else 0.0, mid_b if j == 0 else 0.0)
-        near = jnp.where(ahead_lane, cum_f, cum_b)
-        at = slice(j * blk, (j + 1) * blk)
-        cum = near + far
-        cum_ref[at, :] = jnp.exp(cum)
-        fac_ref[at, :] = rates[j] * jnp.exp(total - cum)
-        col_ref[at, :] = cum
-        cum_t[:, at] = cum.T
-        rate_t[:, at] = rates[j].T
-        mid = rates[j] * jnp.exp(jnp.minimum((mid_f if j == 0 else mid_b) - near, 0.0))
-        mid_t[:, at] = mid.T
-
-    gain_load.wait()
-    gain_ref[...] = gain_in[...].astype(F32)
+    pltpu.make_async_copy(inc.at[core], inc.at[core], load_sem.at[11]).wait()
+    remote(inc_out, inc.at[other], inc_sem.at[0], inc_sem.at[1], partner).wait_recv()
 
     def half_wait(i):
         remote(
@@ -907,8 +849,8 @@
     def up_copy(k, d, i):
         qy, qx, q = member(i)
         return remote(
-            sup.at[k, q, d], up_in.at[k, me, d], up_sem.at[0, 2 * k + d, i],
-            up_sem.at[1, 2 * k + d, me], quad_id(qy, qx),
+            sup.at[k, q, d], up_in.at[k, me, d], up_sem.at[0], up_sem.at[1 + 2 * k + d],
+            quad_id(qy, qx),
         )
 
     def wide_left(n):
@@ -971,26 +913,22 @@
 
     def zlog_copy(o):
         return remote(
-            zsum, zlog.at[cz], zlog_sem.at[0, o], zlog_sem.at[1, cz], z_id(lax.rem(cz + o, nz))
+            zsum, zlog.at[cz], zlog_sem.at[0], zlog_sem.at[1], z_id(lax.rem(cz + o, nz))
         )
 
-    def lanes_of(log_row, d, k):
-        return two(rolled(log_row, me), d * hh + 2 * k)
-
     def quad_logs():
-        for i in range(3):
-            _, _, q = member(i)
-            remote(
-                logs, qlog.at[q], qlog_sem.at[0, i], qlog_sem.at[1, q], partner
-            ).wait_recv()
+        three = qlog.at[0:3]
+        remote(three, three, qlog_sem.at[0], qlog_sem.at[1], partner).wait_recv()
         zsum[...] = qlog[0] + qlog[1] + qlog[2] + qlog[3]
         for o in range(1, nz):
             zlog_copy(o).start()
         zlog[cz] = zsum[...]
+        all_of = rolled(zsum[...], me)
+        each_of = [rolled(qlog[q], me) for q in range(4)]
         for d in range(2):
             for k in range(tiles):
-                zdec[d, k] = jnp.exp(lanes_of(zsum[...], d, k))
-                each = [lanes_of(qlog[q], d, k) for q in range(4)]
+                zdec[d, k] = jnp.exp(two(all_of, d * hh + 2 * k))
+                each = [two(one, d * hh + 2 * k) for one in each_of]
                 reach = jnp.zeros_like(each[0])
                 for q in reversed(range(4)) if d == 0 else range(4):
                     dec[q, d, k] = jnp.exp(each[q])
@@ -998,11 +936,8 @@
                     reach = reach + each[q]
 
     def z_logs():
-        for o in range(1, nz):
-            s = lax.rem(cz + o, nz)
-            remote(
-                zsum, zlog.at[s], zlog_sem.at[0, o], zlog_sem.at[1, s], partner
-            ).wait_recv()
+        rest = zlog.at[0 : nz - 1]
+        remote(rest, rest, zlog_sem.at[0], zlog_sem.at[1], partner).wait_recv()
         reach = [[jnp.zeros((8, 128), F32) for _ in range(2)] for _ in range(rounds)]
         for s in range(nz):
             for r in range(rounds):
@@ -1014,17 +949,14 @@
                 reach[r][0] = reach[r][0] + jnp.where(f_in, zlog[s], 0.0)
                 reach[r][1] = reach[r][1] + jnp.where(b_in, zlog[s], 0.0)
         for d in range(2):
-            for k in range(tiles):
-                for r in range(rounds):
-                    zwt[r, d, k] = jnp.exp(lanes_of(reach[r][d], d, k))
+            for r in range(rounds):
+                total = rolled(reach[r][d], me)
+                for k in range(tiles):
+                    zwt[r, d, k] = jnp.exp(two(total, d * hh + 2 * k))
 
     def combine(k, d):
-        for i in range(3):
-            _, _, q = member(i)
-            remote(
-                sup.at[k, q, d], up_in.at[k, q, d], up_sem.at[0, 2 * k + d, i],
-                up_sem.at[1, 2 * k + d, q], partner,
-            ).wait_recv()
+        three = up_in.at[k, 0:3, d]
+        remote(three, three, up_sem.at[0], up_sem.at[1 + 2 * k + d], partner).wait_recv()
         acc = up_in[k, 0, d].astype(F32) * wup[0, d, k, 0:1, :]
         for q in range(1, 4):
             acc = acc + up_in[k, q, d].astype(F32) * wup[q, d, k, 0:1, :]
@@ -1034,7 +966,7 @@
 
     def z_copy(r, k, o, d):
         return remote(
-            zs.at[r, k], zr.at[r, k], zsend_sem.at[r, k, o - 1], zrecv_sem.at[r, k],
+            zs.at[r, k], zr.at[r, k], zsend_sem.at[r, o - 1], zrecv_sem.at[r, k],
             z_id(cz + o if d == 0 else cz - o),
         )
 
@@ -1058,7 +990,7 @@
         @pl.when(pos >= h if d == 0 else pos < h)
         def _():
             remote(
-                zs.at[r, k], zr.at[r, k], zsend_sem.at[r, k, 0], zrecv_sem.at[r, k], partner
+                zs.at[r, k], zr.at[r, k], zsend_sem.at[r, 0], zrecv_sem.at[r, k], partner
             ).wait_recv()
             zin[k, d] = zin[k, d] + zr[r, k].astype(F32) * zwt[r, d, k, 0:1, :]
 
@@ -1070,8 +1002,8 @@
     def down_copy(k, d, i):
         qy, qx, q = member(i)
         return remote(
-            down_out.at[k, q, d], down_in.at[k, me, d], down_sem.at[0, 2 * k + d, i],
-            down_sem.at[1, 2 * k + d, me], quad_id(qy, qx),
+            down_out.at[k, q, d], down_in.at[k, me, d], down_sem.at[0], down_sem.at[1 + k],
+            quad_id(qy, qx),
         )
 
     def down(k, d):
@@ -1103,7 +1035,7 @@
 
     def mix_copy(k):
         return remote(
-            mix_out.at[k], mix_in.at[k], mix_sem.at[0, k], mix_sem.at[1, k], partner
+            mix_out.at[k], mix_in.at[k], mix_sem.at[0], mix_sem.at[1 + k], partner
         )
 
     def spread(k, ref=cum_ref):
@@ -1115,13 +1047,8 @@
                     wide_cum[k, p, d, j * blk : (j + 1) * blk, :] = two(cols, d * hh + head)
 
     def last(k):
-        for i in range(3):
-            _, _, q = member(i)
-            for d in range(2):
-                remote(
-                    down_out.at[k, q, d], down_in.at[k, q, d], down_sem.at[0, 2 * k + d, i],
-                    down_sem.at[1, 2 * k + d, q], partner,
-                ).wait_recv()
+        three = down_in.at[k, 0:3]
+        remote(three, three, down_sem.at[0], down_sem.at[1 + k], partner).wait_recv()
         for mine in (False, True):
             rows = pl.ds(pl.multiple_of((core if mine else other) * blk, 128), blk)
             for p in range(hp):
@@ -1146,17 +1073,107 @@
         for p in range(hp):
             gate(mix_in[k, p], other * tiles_of[0] + p * tiles + k)
 
-    for spot in range(2 * hp):
-        work[spot, 0:8, :] = jnp.zeros((8, 128), F32)
-        work[spot, 8 + tokens :, :] = jnp.zeros((8, 128), F32)
-    low_ref[...] = jnp.zeros_like(low_ref)
-    high_ref[...] = jnp.zeros_like(high_ref)
+    def early_sent():
+        for x in range(2):
+
+            @pl.when(x * 2 + holder != here)
+            def _(x=x):
+                for i in range(5):
+                    param_copy(i, x).wait_send()
+
+        for low, sends in ((True, sends_low), (False, sends_high)):
+
+            @pl.when(sends)
+            def _(low=low):
+                for k in range(2):
+                    edge_copy(low, k).wait_send()
+
+        inc_copy.wait_send()
+        for i in range(3):
+            half_copy(i).wait_send()
+        for all_of, sem in ((qlog.at[0:3], qlog_sem), (zlog.at[0 : nz - 1], zlog_sem)):
+            remote(all_of, all_of, sem.at[0], sem.at[1], partner).wait_send()
+        sent = sup.at[:, 0:3]
+        remote(sent, sent, up_sem.at[0], up_sem.at[1], partner).wait_send()
+
+    def z_sent():
+        for r in range(rounds):
+            h, _, senders = z_parts(r)
+
+            @pl.when(jnp.logical_or(senders[0][1], senders[1][1]))
+            def _(r=r, h=h):
+                for o in range(h):
+                    remote(
+                        zs.at[r], zr.at[r], zsend_sem.at[r, o], zrecv_sem.at[r, 0], partner
+                    ).wait_send()
+
+    def rest_sent():
+        sent = down_out.at[:, 0:3]
+        remote(sent, sent, down_sem.at[0], down_sem.at[1], partner).wait_send()
+        remote(mix_out, mix_in, mix_sem.at[0], mix_sem.at[1], partner).wait_send()
+
+    half_wait(1)
+    half_wait(0)
+    prm_ref[...] = jnp.zeros_like(prm_ref)
+    wide = own[3].shape[1]
+    for q in range(2):
+        for kind in range(2):
+            for d in range(2):
+                at = slice(d * hh + q * wide, d * hh + (q + 1) * wide)
+                prm_ref[kind : kind + 1, at] = got[3 + kind][q, d : d + 1, :]
+        off = 0
+        for i in range(3):
+            n = own[i].shape[1]
+            part = got[i][q].astype(F32)
+            for t in range(n // 128):
+                w_ref[off + q * (n // 128) + t, 0:4, :] = part[:, t * 128 : (t + 1) * 128]
+            off += 2 * n // 128
+
+    cums, rates = [], []
+    for j in range(2):
+        pre = jnp.concatenate([inc[j, 0], inc[j, 1], filler], axis=0).T
+        spikes = jnp.concatenate([inc[j, 2], inc[j, 2], filler], axis=0).T
+        rate = jax.nn.softplus(pre + prm_ref[0:1, :])
+        log_decay = -jnp.exp(prm_ref[1:2, :]) * rate + spikes
+        cum_f = jnp.dot(lower, log_decay, precision=HIGHEST, preferred_element_type=F32)
+        cum_b = jnp.dot(upper, log_decay, precision=HIGHEST, preferred_element_type=F32)
+        cums.append((cum_f, cum_b))
+        rates.append(rate)
+    ahead_lane = lane < hh
+    ahead1 = ahead_lane[0:1]
+    mid_f, mid_b = cums[0][0][blk - 1 : blk], cums[1][1][0:1]
+    total = jnp.where(ahead1, mid_f + cums[1][0][blk - 1 : blk], cums[0][1][0:1] + mid_b)
+    logs[...] = jnp.broadcast_to(total, (8, 128))
+
+    for j in range(2):
+        cum_f, cum_b = cums[j]
+        far = jnp.where(ahead_lane, mid_f if j == 1 else 0.0, mid_b if j == 0 else 0.0)
+        near = jnp.where(ahead_lane, cum_f, cum_b)
+        at = slice(j * blk, (j + 1) * blk)
+        cum = near + far
+        cum_ref[at, :] = jnp.exp(cum)
+        fac_ref[at, :] = rates[j] * jnp.exp(total - cum)
+        col_ref[at, :] = cum
+        cum_t[:, at] = cum.T
+        rate_t[:, at] = rates[j].T
+        mid = rates[j] * jnp.exp(jnp.minimum((mid_f if j == 0 else mid_b) - near, 0.0))
+        mid_t[:, at] = mid.T
+
+    spread(0, fac_ref)
+    conv(1, 0, 0)
+    conv(0, 0, hp)
+    def qlog_copy(i):
+        qy, qx, q = member(i)
+        return remote(
+            logs, qlog.at[me], qlog_sem.at[0], qlog_sem.at[1], quad_id(qy, qx)
+        )
+
+    for i in range(3):
+        qlog_copy(i).start()
+    qlog[me] = logs[...]
+    gain_load.wait()
+    gain_ref[...] = gain_in[...].astype(F32)
     half_copy(2).start()
-    spread(0, fac_ref)
-    half_wait(1)
-    conv(1, 0, 0)
-    half_wait(0)
-    conv(0, 0, hp)
     edge_wait()
     fix(1, 0)
     fix(0, 0)
@@ -1189,57 +1206,27 @@
                 plan.append((when + z_first + r * z_next, functools.partial(z_recv, r, k, d)))
     for p in range(hp):
         for r in range(2):
-            plan.append((up_step * p + 0.1 + 0.01 * r, functools.partial(inner, p, r)))
+            when = up_step * max(2 * p + r - 1, 0) + 0.1 if p < 3 else up_step * 5 + 0.1
+            plan.append((when, functools.partial(inner, p, r)))
     all_gates = functools.partial(
         lax.fori_loop, 0, 2 * tiles_of[0] // 4, gates, 0
     )
-    plan.append((up_step * hp + 0.1, all_gates))
+    plan.append((up_step * 6 + 0.1, all_gates))
     done = z_first + (rounds - 1) * z_next
-    for k in range(3):
-        plan.append((done + up_step * k + 0.1, functools.partial(spread, k)))
+    plan.append((up_step * 7 + 0.1, functools.partial(spread, 0)))
     for _, step in sorted(plan, key=lambda one: one[0]):
         step()
+    spread(1)
     last(0)
+    spread(2)
+    early_sent()
     last(1)
     finish(0)
+    z_sent()
     last(2)
     finish(1)
     finish(2)
-
-    for x in range(2):
-
-        @pl.when(x * 2 + holder != here)
-        def _(x=x):
-            for i in range(5):
-                param_copy(i, x).wait_send()
-
-    for low, sends in ((True, sends_low), (False, sends_high)):
-
-        @pl.when(sends)
-        def _(low=low):
-            for k in range(2):
-                edge_copy(low, k).wait_send()
-
-    for i in range(3):
-        inc_copy(i).wait_send()
-        half_copy(i).wait_send()
-        qlog_copy(i).wait_send()
-    for o in range(1, nz):
-        zlog_copy(o).wait_send()
-    for k in range(3):
-        for i in range(3):
-            for d in range(2):
-                up_copy(k, d, i).wait_send()
-                down_copy(k, d, i).wait_send()
-        mix_copy(k).wait_send()
-        for r in range(rounds):
-            h, _, senders = z_parts(r)
-            for d, sender in senders:
-
-                @pl.when(sender)
-                def _(k=k, r=r, d=d, h=h):
-                    for o in range(1, h + 1):
-                        z_copy(r, k, o, d).wait_send()
+    rest_sent()
 
 
 def fits_quad(sp, dp, blk, heads, groups):
@@ -1287,9 +1274,9 @@
     scratch += [vm((tiles, 2, STATE, 128), F32)] * 2 + [vm((rounds, tiles, STATE, 128), BF16)] * 2
     scratch += [vm((tiles, hp, blk, 128), BF16)] * 2
     dma = pltpu.SemaphoreType.DMA
-    scratch += [dma((16,)), dma((2, 5, 2)), dma((2, 2)), dma((2, 3)), dma((2, 3))]
-    scratch += [dma((2, 4)), dma((2, nz)), dma((2, 2 * tiles, 4)), dma((rounds, tiles, nz))]
-    scratch += [dma((rounds, tiles)), dma((2, 2 * tiles, 4)), dma((2, tiles))]
+    scratch += [dma((12,)), dma((2, 5, 2)), dma((2, 2)), dma((2, 3)), dma((2,))]
+    scratch += [dma((2,)), dma((2,)), dma((1 + 2 * tiles,)), dma((rounds, nz // 2))]
+    scratch += [dma((rounds, tiles)), dma((1 + tiles,)), dma((1 + tiles,))]
     out = pl.pallas_call(
         functools.partial(quad_kernel, (heads, pairs, sp, dp)),
         out_shape=pltpu.VMEM((blk, x_total), BF16),

time: 36.1 us -> 34.2 us (0.947)
  Pallas kernels: 34.8 us -> 33 us
    pallas_call x1, Pallas kernels: 34.8 us -> 33 us  [quad_local(): pl.pallas_call(functools.partial(quad_kernel, (heads, pairs, sp, dp)), ou...]
where the time goes in v5:
time: 34.2 us; the launch traced here: 33.9 us
  Pallas kernels  33 us (96%)
  local copies, waits for them, and re-layouts  0.88 us (3%)
    pallas_call x1, Pallas kernels, quad_local(): pl.pallas_call(functools.partial(quad_kernel, (heads, pairs, sp, dp)), ou...  33 us
    unnamed x1, local copies, waits for them, and re-layouts  0.88 us

profile of v5, /device:TPU:0, one launch (start us, length us, event | category | flops | bytes accessed | tf_op | source)
XLA Modules:
  0.0 33.9 jit_solution(1292593424510614200)
XLA Ops:
  0.0 33.0 %mixer.1 = bf16[128,3072]{1,0:T(8,128)(2,1)S(1)} custom-call(bf16[128,3072]{1,0:T(8,128)(2,1)} %bitcast.16, bf16[128,2048]{1,0:T(8,128)(2,1)} %bitcast.18, bf16[128,2048]{1,0:T(8,128)(2,1)} %bitcast.19, bf16[128,3072]{1,0:T(8,128)(2,1)} %bitcast.17, f32[48,128]{1,0:T(8,128)} %bitcast.20, f32[48,128]{1,0:T(8,128)} %bitcast.21, f32[48,128]{1,0:T(8,128)} %bitcast.22, ...), custom_call_target="tpu_custom_call" | custom-call | tf_op jit(solution)/shard_map/mixer/pallas_call | solution.py:1280
  33.0 0.9 %copy.15 = bf16[1,128,3072]{2,1,0:T(8,128)(2,1)} copy(bf16[1,128,3072]{2,1,0:T(8,128)(2,1)S(1)} %bitcast.15) | data formatting | bytes 1572864

commit v6 on v5

--- a/solution.py
+++ b/solution.py
@@ -658,8 +658,6 @@
     b_load = load(b_hbm, in_b)
     x_load = load(x_hbm, in_x)
     c_load = load(c_hbm, in_c)
-    gain_load = load(gain_hbm, gain_in)
-    z_load = load(z_hbm, in_z)
 
     for spot in range(2 * hp):
         work[spot, 0:8, :] = jnp.zeros((8, 128), F32)
@@ -742,6 +740,8 @@
 
     for i in (1, 0):
         half_copy(i).start()
+    gain_load = load(gain_hbm, gain_in)
+    z_load = load(z_hbm, in_z)
 
     lane = lax.broadcasted_iota(jnp.int32, (blk, 128), 1)
     row = lax.broadcasted_iota(jnp.int32, (blk, 128), 0)
@@ -1189,15 +1189,18 @@
     fix(0, 2)
     first(2)
     quad_logs()
-    half_wait(2)
-    for k in range(2):
-        conv(2, k, k * hp)
-    for k in range(2):
-        fix(2, k)
+
+    def ready_c():
+        half_wait(2)
+        for k in range(2):
+            conv(2, k, k * hp)
+        for k in range(2):
+            fix(2, k)
+
     z_load.wait()
 
     up_step, z_first, z_next = 1.4, 2.7, 3.5
-    plan = [(z_first - 0.01, z_logs)]
+    plan = [(z_first - 0.01, z_logs), (0.05, ready_c)]
     for k in range(3):
         for d in range(2):
             when = up_step * (2 * k + d)
@@ -1206,14 +1209,14 @@
                 plan.append((when + z_first + r * z_next, functools.partial(z_recv, r, k, d)))
     for p in range(hp):
         for r in range(2):
-            when = up_step * max(2 * p + r - 1, 0) + 0.1 if p < 3 else up_step * 5 + 0.1
+            when = up_step * (2 * p + r) + 0.1
             plan.append((when, functools.partial(inner, p, r)))
     all_gates = functools.partial(
         lax.fori_loop, 0, 2 * tiles_of[0] // 4, gates, 0
     )
-    plan.append((up_step * 6 + 0.1, all_gates))
+    plan.append((up_step * 8 + 0.1, all_gates))
     done = z_first + (rounds - 1) * z_next
-    plan.append((up_step * 7 + 0.1, functools.partial(spread, 0)))
+    plan.append((up_step * 9 + 0.1, functools.partial(spread, 0)))
     for _, step in sorted(plan, key=lambda one: one[0]):
         step()
     spread(1)

time: 34.2 us -> 34 us (level)
  no operation moved by 1% of the time
where the time goes in v6:
time: 34 us; the launch traced here: 33.7 us
  Pallas kernels  32.8 us (96%)
  local copies, waits for them, and re-layouts  0.88 us (3%)
    pallas_call x1, Pallas kernels, quad_local(): pl.pallas_call(functools.partial(quad_kernel, (heads, pairs, sp, dp)), ou...  32.8 us
    unnamed x1, local copies, waits for them, and re-layouts  0.88 us

profile of v6, /device:TPU:0, one launch (start us, length us, event | category | flops | bytes accessed | tf_op | source)
XLA Modules:
  0.0 33.7 jit_solution(10629389949394880551)
XLA Ops:
  0.0 32.8 %mixer.1 = bf16[128,3072]{1,0:T(8,128)(2,1)S(1)} custom-call(bf16[128,3072]{1,0:T(8,128)(2,1)} %bitcast.16, bf16[128,2048]{1,0:T(8,128)(2,1)} %bitcast.18, bf16[128,2048]{1,0:T(8,128)(2,1)} %bitcast.19, bf16[128,3072]{1,0:T(8,128)(2,1)} %bitcast.17, f32[48,128]{1,0:T(8,128)} %bitcast.20, f32[48,128]{1,0:T(8,128)} %bitcast.21, f32[48,128]{1,0:T(8,128)} %bitcast.22, ...), custom_call_target="tpu_custom_call" | custom-call | tf_op jit(solution)/shard_map/mixer/pallas_call | solution.py:1283
  32.8 0.9 %copy.15 = bf16[1,128,3072]{2,1,0:T(8,128)(2,1)} copy(bf16[1,128,3072]{2,1,0:T(8,128)(2,1)S(1)} %bitcast.15) | data formatting | bytes 1572864
